TPU v7x, 32 devices: a whole 2x2x4 slice. The times are simulated.
32 devices in a mesh: sp: 8 (over z, x), tp: 4 (over y, core).
Axes of the slice: x: 2, y: 2, z: 4, core: 2. Of those that a mesh axis runs over, the one named last changes fastest.
Arguments:
- tokens_in: bfloat16 [6144, 2048], P(('sp', 'tp')), may hold values from -300 to 300
- norm_gain: float32 [2048], replicated, may hold values from 0.1 to 1.9
- query_weight: bfloat16 [2048, 1024], P('sp', 'tp'), may hold values from -64 to 64
- key_weight: bfloat16 [2048, 512], P('sp', 'tp'), may hold values from -1 to 1
- value_weight: bfloat16 [2048, 512], P('sp', 'tp'), may hold values from -0.125 to 0.125
- pool_weight: bfloat16 [2048, 1024], P('sp', 'tp'), may hold values from -0.125 to 0.125
- sink_logit: float32 [16], P('tp'), may hold values from 1 to 5
- pool_gain: float32 [1024], P('tp'), may hold values from 0.1 to 1.9
- attention_out_weight: bfloat16 [1024, 2048], P('tp', 'sp'), may hold values from -0.125 to 0.125
- pool_out_weight: bfloat16 [1024, 2048], P('tp', 'sp'), may hold values from -0.1875 to 0.1875
Outputs:
- mixed_out: bfloat16 [6144, 2048], P(('sp', 'tp'))
All inputs are finite; a program needn't handle non-finite values.
Results may differ from a plain program's by a relative error of at most 0.014.
Values may be sent and summed in bfloat16 or wider, within the bound.
A program may use at most 64 MiB of HBM per device.

v0:
```python
import functools
import math

import jax
import jax.numpy as jnp
from jax import lax
from jax.experimental import pallas as pl
from jax.experimental.pallas import tpu as pltpu
from jax.sharding import PartitionSpec as P

HEAD_DIM = 64
POOL_CH = 256
POOL_GROUPS = 4
WINDOW = 128
EPS = 1e-06
SHORT_REACHES = (8, 32)
CORES = 2
SIDE_SHARE = 0.3
MESH = pl.DeviceIdType.MESH
F32 = jnp.float32
BF16 = jnp.bfloat16


def row_tile(rows, most):
    tile = most
    while rows % tile:
        tile -= 16
    return tile


def kernel(n_sp, n_tp, cols, n_in, n_out, widths, *refs):
    tok, gain, sink, pgain = refs[:4]
    win_refs = refs[4 : 4 + n_in]
    wout_refs = refs[4 + n_in : 4 + n_in + n_out]
    (
        out, tokv, xs, wq, wp, wo, accq, accp, ext, mix, tot, carry, dsend, drecv, ysend, yrecv, own,
        local_sem, send_sem, sem_q, sem_p, sem_p_side, sem_out, sem_out_side,
        sem_tok, sem_halo, sem_tot, sem_core, sem_y,
    ) = refs[4 + n_in + n_out :]
    qw, kw, vw, pw = widths
    levels = n_sp // cols
    chips = n_tp // CORES
    rows, seq = tok.shape[0], xs.shape[1]
    qkv = wq.shape[2]
    piece = xs.shape[2]
    blocks = seq // WINDOW
    me, t = lax.axis_index("sp"), lax.axis_index("tp")
    z, x = me // cols, me % cols
    y, c = t // CORES, t % CORES
    partner = y * CORES + (1 - c)

    locals_ = []
    at = 0
    for i, ref in enumerate(win_refs[:-1]):
        w = ref.shape[1]
        locals_.append(pltpu.make_async_copy(ref, wq.at[me, :, pl.ds(at, w)], local_sem.at[i]))
        at += w
    locals_.append(pltpu.make_async_copy(win_refs[-1], wp.at[me], local_sem.at[n_in - 1]))
    at = 0
    for i, ref in enumerate(wout_refs):
        k = ref.shape[0]
        locals_.append(
            pltpu.make_async_copy(ref, wo.at[me, pl.ds(at, k), :], local_sem.at[n_in + i])
        )
        at += k
    tok_copy = pltpu.make_async_copy(tok, tokv, local_sem.at[n_in + n_out])
    for copy in locals_[:n_in] + [tok_copy] + locals_[n_in:]:
        copy.start()

    barrier = pltpu.get_barrier_semaphore()
    for d in range(1, n_sp):
        pl.semaphore_signal(barrier, inc=1, device_id=((me + d) % n_sp, t), device_id_type=MESH)
    for d in range(1, n_tp):
        pl.semaphore_signal(barrier, inc=1, device_id=(me, (t + d) % n_tp), device_id_type=MESH)
    pl.semaphore_wait(barrier, n_sp + n_tp - 2)

    sent = []

    def when(cond, fn):
        if cond is None:
            fn()
        else:
            pl.when(cond)(fn)

    def both(a, b):
        return b if a is None else (a if b is None else jnp.logical_and(a, b))

    def send(cond, src, dst, recv, dev):
        copy = pltpu.make_async_remote_copy(
            src_ref=src, dst_ref=dst, send_sem=send_sem.at[len(sent)], recv_sem=recv,
            device_id=dev, device_id_type=MESH,
        )
        when(cond, copy.start)
        sent.append((cond, copy))

    def arrived(cond, dst, recv):
        copy = pltpu.make_async_remote_copy(
            src_ref=dst, dst_ref=dst, send_sem=send_sem.at[0], recv_sem=recv,
            device_id=(me, partner), device_id_type=MESH,
        )
        when(cond, copy.wait_recv)

    up, down = z + 1 < levels, z > 0

    class Spread:
        def __init__(self, buf, main_sem, side_sem):
            self.buf, self.main_sem, self.side_sem = buf, main_sem, side_sem
            k = buf.shape[1]
            self.side = 0 if side_sem is None else max(16, int(k * SIDE_SHARE) // 16 * 16)
            self.main = k - self.side

        def part(self, s, which):
            if which == "all":
                return self.buf.at[s]
            if which == "main":
                return self.buf.at[s, pl.ds(0, self.main), :]
            return self.buf.at[s, pl.ds(self.main, self.side), :]

        def go(self, cond, s, which, dev_sp):
            if which == "side" and not self.side:
                return
            sem = self.side_sem if which == "side" else self.main_sem
            ref = self.part(s, which)
            send(cond, ref, ref, sem.at[s], (dev_sp, t))

        def across(self, cond, s, which):
            for d in range(1, cols):
                self.go(cond, s, which, z * cols + (x + d) % cols)

        def peers(self, level):
            return [level * cols + (x + cols - d) % cols for d in range(1, cols)]

        def begin(self):
            self.across(None, me, "side")
            self.go(up, me, "all", me + cols)
            self.go(down, me, "all", me - cols)
            self.across(None, me, "main")

        def begin_side(self):
            for s in self.peers(z) if self.side else []:
                arrived(None, self.part(s, "side"), self.side_sem.at[s])
                self.go(up, s, "side", me + cols)
                self.go(down, s, "side", me - cols)

        def hop(self, h):
            for level, there, on, to in (
                (z - h, z - h >= 0, up, me + cols),
                (z + h, z + h < levels, down, me - cols),
            ):
                s = level * cols + x
                arrived(there, self.part(s, "all"), self.main_sem.at[s])
                self.go(both(there, on), s, "all", to)
                self.across(there, s, "main")
                for s in self.peers(level) if self.side else []:
                    arrived(there, self.part(s, "side"), self.side_sem.at[s])
                    self.go(both(there, on), s, "side", to)

        def ready(self, h):
            found = []
            for level, there in (
                ((z, None),) if h == 0 else ((z - h, z - h >= 0), (z + h, z + h < levels))
            ):
                found.append((there, level * cols + x, None))
                for s in self.peers(level):
                    found.append(
                        (
                            there,
                            s,
                            functools.partial(
                                arrived, None, self.part(s, "main"), self.main_sem.at[s]
                            ),
                        )
                    )
            return found

    spread_q = Spread(wq, sem_q, None)
    spread_p = Spread(wp, sem_p, sem_p_side)
    spread_out = Spread(wo, sem_out, sem_out_side)
    for copy in locals_[:n_in]:
        copy.wait()
    spread_q.begin()
    spread_p.begin()
    tok_copy.wait()

    mine = pl.ds(pl.multiple_of(t * rows, rows), rows)
    wide = tokv[...].astype(F32)
    inverse = lax.rsqrt(jnp.mean(wide * wide, axis=1, keepdims=True) + EPS)
    for i in range(n_sp):
        span = slice(i * piece, (i + 1) * piece)
        xs[i, mine, :] = (tokv[:, span].astype(F32) * inverse * gain[:, span]).astype(BF16)

    def rows_of(device):
        return xs.at[:, pl.ds(pl.multiple_of(device * rows, rows), rows), :]

    for d in range(1, chips):
        send(None, rows_of(t), rows_of(t), sem_tok.at[t], (me, (y + d) % chips * CORES + c))
    send(None, rows_of(t), rows_of(t), sem_tok.at[t], (me, partner))

    for h in range(1, levels - 1):
        spread_q.hop(h)
    spread_p.begin_side()
    for h in range(1, levels - 2):
        spread_p.hop(h)

    for d in range(1, chips):
        far = (y + chips - d) % chips * CORES + c
        arrived(None, rows_of(far), sem_tok.at[far])
        send(None, rows_of(far), rows_of(far), sem_tok.at[far], (me, partner))
    arrived(None, rows_of(partner), sem_tok.at[partner])
    for d in range(1, chips):
        far = (y + chips - d) % chips * CORES + (1 - c)
        arrived(None, rows_of(far), sem_tok.at[far])

    spread_q.hop(levels - 1)
    for h in range(max(1, levels - 2), levels - 1):
        spread_p.hop(h)
    for copy in locals_[n_in:]:
        copy.wait()
    spread_out.begin()

    tile = row_tile(seq, 256)

    def project(spread, acc, h):
        for i, (cond, s, wait) in enumerate(spread.ready(h)):

            def run(s=s, wait=wait, first=(h == 0 and i == 0)):
                if wait is not None:
                    wait()

                @pl.loop(0, seq // tile)
                def _(i):
                    r = pl.ds(pl.multiple_of(i * tile, tile), tile)
                    value = jnp.dot(xs[s, r, :], spread.buf[s], preferred_element_type=F32)
                    if first:
                        acc[r, :] = value
                    else:
                        acc[r, :] += value

            when(cond, run)

    def settle(acc, at):
        @pl.loop(0, seq // tile)
        def _(i):
            r = pl.multiple_of(i * tile, tile)
            to = pl.ds(pl.multiple_of(r + WINDOW, WINDOW), tile)
            ext[to, at : at + acc.shape[1]] = acc[pl.ds(r, tile), :].astype(BF16)

    later, earlier = me + 1 < n_sp, me > 0

    def pass_on(at, width, i):
        head = ext.at[pl.ds(0, WINDOW), pl.ds(at, width)]
        tail = ext.at[pl.ds(seq, WINDOW), pl.ds(at, width)]
        send(later, tail, head, sem_halo.at[i], (me + 1, t))
        return head

    for h in range(levels - 1):
        project(spread_q, accq, h)
    spread_p.hop(levels - 1)
    project(spread_q, accq, levels - 1)
    settle(accq, 0)
    head_kv = pass_on(qw, kw + vw, 0)
    channel0 = qkv
    group = t * pw // POOL_CH
    whole_prefix = group == POOL_GROUPS - 1

    group_heads = qw // kw
    stacked = group_heads * WINDOW
    scale = HEAD_DIM ** (-0.5)

    def attend(n):
        q_rows = pl.ds(pl.multiple_of(n * WINDOW + WINDOW, WINDOW), WINDOW)
        k_rows = pl.ds(pl.multiple_of(n * WINDOW, WINDOW), 2 * WINDOW)
        queries = ext[q_rows, :qw]
        keys = ext[k_rows, qw : qw + kw]
        values = ext[k_rows, qw + kw : channel0]
        row = lax.broadcasted_iota(jnp.int32, (stacked, 2 * WINDOW), 0)
        q_index = row % WINDOW
        k_index = lax.broadcasted_iota(jnp.int32, (stacked, 2 * WINDOW), 1)
        lowest = jnp.where(me * blocks + n == 0, WINDOW, 0)
        allowed = (k_index > q_index) & (k_index <= q_index + WINDOW) & (k_index >= lowest)
        which = lax.broadcasted_iota(jnp.int32, (stacked, 1), 0) // WINDOW
        done = []
        for j in range(kw // HEAD_DIM):
            part = slice(j * HEAD_DIM, (j + 1) * HEAD_DIM)
            first = j * group_heads
            q = jnp.concatenate(
                [
                    queries[:, (first + g) * HEAD_DIM : (first + g + 1) * HEAD_DIM]
                    for g in range(group_heads)
                ],
                axis=0,
            )
            scores = (
                lax.dot_general(
                    q, keys[:, part], (((1,), (1,)), ((), ())), preferred_element_type=F32
                )
                * scale
            )
            scores = jnp.where(allowed, scores, -jnp.inf)
            sinks = jnp.full((stacked, 1), sink[first], F32)
            for g in range(1, group_heads):
                sinks = jnp.where(which == g, sink[first + g], sinks)
            peak = jnp.maximum(jnp.max(scores, axis=1, keepdims=True), sinks)
            expo = jnp.exp(scores - peak)
            denom = jnp.sum(expo, axis=1, keepdims=True) + jnp.exp(sinks - peak)
            probs = (expo * (1.0 / denom)).astype(BF16)
            got = jnp.dot(probs, values[:, part], preferred_element_type=F32)
            done += [got[g * WINDOW : (g + 1) * WINDOW] for g in range(group_heads)]
        to = pl.ds(pl.multiple_of(n * WINDOW, WINDOW), WINDOW)
        mix[to, :qw] = jnp.concatenate(done, axis=1).astype(BF16)

    spread_out.begin_side()
    spread_out.hop(1)
    third = max(2, (blocks + 1) // 2)
    pl.loop(1, third)(attend)
    for h in range(levels):
        project(spread_p, accp, h)
    settle(accp, channel0)
    head_pool = pass_on(channel0, pw, 1)
    total = jnp.sum(ext[WINDOW:, channel0:].astype(F32), axis=0, keepdims=True)
    tot[me] = jnp.broadcast_to(total, tot.shape[1:])
    for d in range(1, n_sp):
        send(
            both(whole_prefix, me + d < n_sp), tot.at[me], tot.at[me], sem_tot.at[me],
            (me + d, t),
        )
    pl.loop(third, blocks)(attend)

    @pl.when(jnp.logical_not(earlier))
    def _():
        ext[:WINDOW, qw:] = jnp.zeros((WINDOW, ext.shape[1] - qw), BF16)

    arrived(earlier, head_kv, sem_halo.at[0])
    attend(0)
    for h in range(2, levels - 1):
        spread_out.hop(h)
    arrived(earlier, head_pool, sem_halo.at[1])

    carry[...] = jnp.zeros(carry.shape, F32)
    for d in range(1, n_sp):

        def add(d=d):
            arrived(None, tot.at[me - d], sem_tot.at[me - d])
            carry[...] += tot[me - d]

        when(both(whole_prefix, me - d >= 0), add)

    reach = jnp.where(
        group == 0, SHORT_REACHES[0], jnp.where(group == 1, SHORT_REACHES[1], WINDOW)
    )
    reach = jnp.where(whole_prefix, n_sp * seq, reach)
    lowest = jnp.where(whole_prefix, WINDOW, 0)

    @pl.loop(0, blocks)
    def _(n):
        q_index = lax.broadcasted_iota(jnp.int32, (WINDOW, 2 * WINDOW), 0)
        k_index = lax.broadcasted_iota(jnp.int32, (WINDOW, 2 * WINDOW), 1)
        distance = q_index + WINDOW - k_index
        band = (distance >= 0) & (distance < reach) & (k_index >= lowest)
        band = jnp.where(band, 1.0, 0.0).astype(BF16)
        k_rows = pl.ds(pl.multiple_of(n * WINDOW, WINDOW), 2 * WINDOW)
        both_blocks = ext[k_rows, channel0:]
        sums = jnp.dot(band, both_blocks, preferred_element_type=F32) + carry[0:1, :]
        position = me * seq + n * WINDOW + lax.broadcasted_iota(jnp.int32, (WINDOW, 1), 0)
        counted = jnp.minimum(position + 1, reach).astype(F32)
        mixed = (sums / counted - both_blocks[WINDOW:].astype(F32)) * pgain[...]
        mix[pl.ds(pl.multiple_of(n * WINDOW, WINDOW), WINDOW), qw:] = mixed.astype(BF16)
        carry[...] = jnp.where(
            whole_prefix, jnp.broadcast_to(sums[WINDOW - 1 :], carry.shape), 0.0
        )

    def mix_rows(chip, core):
        return mix[pl.ds(pl.multiple_of((chip * CORES + core) * rows, rows), rows), :]

    outs = []

    def multiply(cond, s, wait):
        def run():
            if wait is not None:
                wait()
            for chip in range(chips):
                dsend[s, chip] = jnp.dot(
                    mix_rows(chip, 1 - c), wo[s], preferred_element_type=F32
                ).astype(BF16)

        when(cond, run)
        send(cond, dsend.at[s], drecv.at[s], sem_core.at[s], (me, partner))

        def keep():
            for chip in range(chips):
                own[s, chip] = jnp.dot(mix_rows(chip, c), wo[s], preferred_element_type=F32)

        when(cond, keep)

    def finish(cond, s):
        arrived(cond, drecv.at[s], sem_core.at[s])
        for d in range(1, chips):
            far = (y + d) % chips

            def pack(d=d, far=far):
                ysend[s, d - 1] = (own[s, far] + drecv[s, far].astype(F32)).astype(BF16)

            when(cond, pack)
            last.append(len(sent))
            send(
                cond, ysend.at[s, d - 1], yrecv.at[s, d - 1], sem_y.at[s, d - 1],
                (me, far * CORES + c),
            )

    last = []
    pending = None
    for h in range(levels):
        if h == levels - 1:
            if pending is not None:
                finish(*pending)
                pending = None
            spread_out.hop(h)
        for cond, s, wait in spread_out.ready(h):
            multiply(cond, s, wait)
            if pending is not None:
                finish(*pending)
            pending = (cond, s)
    finish(*pending)

    for i, (cond, copy) in enumerate(sent):
        if i not in last:
            when(cond, copy.wait_send)

    for i in range(n_sp):
        value = own[i, y] + drecv[i, y].astype(F32)
        for d in range(1, chips):
            arrived(None, yrecv.at[i, d - 1], sem_y.at[i, d - 1])
            value += yrecv[i, d - 1].astype(F32)
        w = wo.shape[2]
        out[:, i * w : (i + 1) * w] = value.astype(BF16)

    for i in last:
        when(sent[i][0], sent[i][1].wait_send)


def local(
    n_sp, n_tp, tokens_in, norm_gain, query_weight, key_weight, value_weight, pool_weight,
    sink_logit, pool_gain, attention_out_weight, pool_out_weight,
):
    rows, depth = tokens_in.shape
    seq = rows * n_tp
    ins = [query_weight, key_weight, value_weight, pool_weight]
    outs = [attention_out_weight, pool_out_weight]
    widths = tuple(w.shape[1] for w in ins)
    if any(w % 128 for w in widths):
        ins = [jnp.concatenate(ins[:3], axis=1), ins[3]]
    cols = math.gcd(n_sp, max(1, n_tp // CORES))
    levels, chips = n_sp // cols, n_tp // CORES
    k_in, k_out = ins[0].shape[0], sum(w.shape[0] for w in outs)
    width, out_cols = sum(widths), outs[0].shape[1]
    pw = widths[3]
    hops = 2 * (levels - 1) + 1
    n_send = 3 * (2 + 2 * cols + hops * (2 + 3 * cols)) + 2 * n_tp + n_sp + 2
    n_send += 2 * n_sp * hops * chips
    vmem = pl.BlockSpec(memory_space=pltpu.VMEM)
    hbm = pl.BlockSpec(memory_space=pl.ANY)
    dma = pltpu.SemaphoreType.DMA
    return pl.pallas_call(
        functools.partial(kernel, n_sp, n_tp, cols, len(ins), len(outs), widths),
        out_shape=jax.ShapeDtypeStruct((rows, depth), BF16),
        in_specs=[hbm, vmem, pl.BlockSpec(memory_space=pltpu.SMEM), vmem]
        + [hbm] * (len(ins) + len(outs)),
        out_specs=vmem,
        scratch_shapes=[
            pltpu.VMEM((rows, depth), BF16),
            pltpu.VMEM((n_sp, seq, depth // n_sp), BF16),
            pltpu.VMEM((n_sp, k_in, width - pw), BF16),
            pltpu.VMEM((n_sp, k_in, pw), BF16),
            pltpu.VMEM((n_sp, k_out, out_cols), BF16),
            pltpu.VMEM((seq, width - pw), F32),
            pltpu.VMEM((seq, pw), F32),
            pltpu.VMEM((seq + WINDOW, width), BF16),
            pltpu.VMEM((seq, widths[0] + pw), BF16),
            pltpu.VMEM((n_sp, 8, pw), F32),
            pltpu.VMEM((8, pw), F32),
            pltpu.VMEM((n_sp, chips, rows, out_cols), BF16),
            pltpu.VMEM((n_sp, chips, rows, out_cols), BF16),
            pltpu.VMEM((n_sp, max(1, chips - 1), rows, out_cols), BF16),
            pltpu.VMEM((n_sp, max(1, chips - 1), rows, out_cols), BF16),
            pltpu.VMEM((n_sp, chips, rows, out_cols), F32),
            dma((len(ins) + len(outs) + 1,)),
            dma((n_send,)),
            dma((n_sp,)),
            dma((n_sp,)),
            dma((n_sp,)),
            dma((n_sp,)),
            dma((n_sp,)),
            dma((n_tp,)),
            dma((2,)),
            dma((n_sp,)),
            dma((n_sp,)),
            dma((n_sp, max(1, chips - 1))),
        ],
        compiler_params=pltpu.CompilerParams(
            collective_id=0, has_side_effects=True, vmem_limit_bytes=58 << 20
        ),
    )(
        tokens_in, norm_gain.reshape(1, -1), sink_logit, pool_gain.reshape(1, -1), *ins, *outs
    )


def solution(mesh):
    in_specs = (
        P(("sp", "tp"), None), P(), P("sp", "tp"), P("sp", "tp"), P("sp", "tp"), P("sp", "tp"),
        P("tp"), P("tp"), P("tp", "sp"), P("tp", "sp"),
    )
    out_specs = P(("sp", "tp"), None)
    return jax.shard_map(
        functools.partial(local, mesh.shape["sp"], mesh.shape["tp"]),
        mesh=mesh, in_specs=in_specs, out_specs=out_specs, check_vma=False,
    )
```

profile of v0, /device:TPU:0, one launch (start us, length us, event | category | flops | bytes accessed | tf_op | source)
XLA Modules:
  0.0 85.6 jit_solution(10450331292942494342)
XLA Ops:
  0.0 83.5 %shard_map.100 = bf16[192,2048]{1,0:T(8,128)(2,1)} custom-call(bf16[192,2048]{1,0:T(8,128)(2,1)} %refs_0_.1, f32[1,2048]{1,0:T(1,128)} %bitcast.2, f32[4]{0:T(128)} %refs_2_.1, f32[1,256]{1,0:T(1,128)} %bitcast.3, bf16[256,256]{1,0:T(8,128)(2,1)} %refs_4_.1, bf16[256,128]{1,0:T(8,128)(2,1)} %refs_5_.1, bf16[256,128]{1,0:T(8,128)(2,1)} %refs_6_.1, ...), custom_call_target="tpu_custom_call" | custom-call | tf_op jit(solution)/shard_map/pallas_call | solution.py:463
  83.5 2.1 %copy.12 = bf16[192,2048]{1,0:T(8,128)(2,1)} copy(bf16[192,2048]{1,0:T(8,128)(2,1)} %shard_map.100) | data formatting | bytes 1572864
where the time goes:
time: 85.8 us; the launch traced here: 85.6 us
  Pallas kernels  83.5 us (97%)
  local copies, waits for them, and re-layouts  2.09 us (2%)
    pallas_call x1, Pallas kernels, local(): pl.pallas_call(functools.partial(kernel, n_sp, n_tp, cols, len(ins), len(...  83.5 us
    unnamed x1, local copies, waits for them, and re-layouts  2.09 us

commit v1 on v0

v1 whole, which is shorter than its diff:
```python
import functools
import math

import jax
import jax.numpy as jnp
from jax import lax
from jax.experimental import pallas as pl
from jax.experimental.pallas import tpu as pltpu
from jax.sharding import PartitionSpec as P

HEAD_DIM = 64
POOL_CH = 256
POOL_GROUPS = 4
WINDOW = 128
EPS = 1e-06
SHORT_REACHES = (8, 32)
CORES = 2
SEND_SLOTS = 32
MESH = pl.DeviceIdType.MESH
F32 = jnp.float32
BF16 = jnp.bfloat16


def when(cond, fn):
    if cond is None:
        fn()
    else:
        pl.when(cond)(fn)


def both(a, b):
    return b if a is None else (a if b is None else jnp.logical_and(a, b))


def kernel(n_sp, n_tp, cols, n_in, n_out, widths, *refs):
    tok, gain, sink, pgain = refs[:4]
    win_refs = refs[4 : 4 + n_in]
    wout_refs = refs[4 + n_in : 4 + n_in + n_out]
    (
        out, tokv, xs, wq, wkv, wp, wa, wb, acc, ext, mix, tot, carry, dfar, rfar, dnear, rnear,
        ysend, yrecv, ofar, onear,
        local_sem, send_sem, sem_q, sem_kv, sem_p, sem_a, sem_b, sem_b_side,
        sem_tok, sem_halo, sem_tot, sem_far, sem_near, sem_y,
    ) = refs[4 + n_in + n_out :]
    qw, kw, vw, pw = widths
    levels = n_sp // cols
    chips = n_tp // CORES
    rows, seq = tok.shape[0], xs.shape[1]
    per = rows * CORES
    channel0 = qw + kw + vw
    blocks = seq // WINDOW
    me, t = lax.axis_index("sp"), lax.axis_index("tp")
    z, x = me // cols, me % cols
    y, c = t // CORES, t % CORES
    partner = y * CORES + (1 - c)
    up, down = z + 1 < levels, z > 0
    later, earlier = me + 1 < n_sp, me > 0

    locals_ = []

    def fetch(src, dst):
        copy = pltpu.make_async_copy(src, dst, local_sem.at[len(locals_)])
        copy.start()
        locals_.append(copy)

    fetch(win_refs[0], wq.at[me])
    at = 0
    for ref in win_refs[1:-1]:
        w = ref.shape[1]
        fetch(ref, wkv.at[me, :, pl.ds(at, w)])
        at += w
    fetch(win_refs[-1], wp.at[me])
    fetch(tok, tokv)
    fetch(wout_refs[0], wa.at[me])
    fetch(wout_refs[1], wb.at[me])
    ext[:WINDOW, qw:] = jnp.zeros((WINDOW, ext.shape[1] - qw), BF16)

    barrier = pltpu.get_barrier_semaphore()
    next_row = jnp.logical_and(x == cols - 1, up)
    last_row = jnp.logical_and(x == 0, down)

    def greet(cond, sp, tp):
        when(
            cond,
            lambda: pl.semaphore_signal(
                barrier, inc=1, device_id=(sp, tp), device_id_type=MESH
            ),
        )

    for d in range(1, cols):
        greet(None, z * cols + (x + d) % cols, t)
    greet(up, me + cols, t)
    greet(down, me - cols, t)
    greet_diagonal = cols > 1
    if greet_diagonal:
        greet(next_row, me + 1, t)
        greet(last_row, me - 1, t)
    for d in range(1, n_tp):
        greet(None, me, (t + d) % n_tp)
    expected = cols - 1 + n_tp - 1 + jnp.where(up, 1, 0) + jnp.where(down, 1, 0)
    if greet_diagonal:
        expected = expected + jnp.where(next_row, 1, 0) + jnp.where(last_row, 1, 0)
    with jax.named_scope("barrier"):
        pl.semaphore_wait(barrier, expected)

    slots = [None] * send_sem.shape[0]
    count = [0]

    def send(cond, src, dst, recv, dev):
        slot = count[0] % len(slots)
        count[0] += 1
        if slots[slot] is not None:
            when(slots[slot][0], slots[slot][1].wait_send)
        copy = pltpu.make_async_remote_copy(
            src_ref=src, dst_ref=dst, send_sem=send_sem.at[slot], recv_sem=recv,
            device_id=dev, device_id_type=MESH,
        )
        when(cond, copy.start)
        slots[slot] = (cond, copy)

    def arrived(cond, dst, recv):
        copy = pltpu.make_async_remote_copy(
            src_ref=dst, dst_ref=dst, send_sem=send_sem.at[0], recv_sem=recv,
            device_id=(me, partner), device_id_type=MESH,
        )
        when(cond, copy.wait_recv)

    def at_distance(h):
        if h == 0:
            return ((z, None, None, None),)
        return (
            (z - h, z - h >= 0, up, me + cols),
            (z + h, z + h < levels, down, me - cols),
        )

    class Spread:
        def __init__(self, name, buf, sem, share=0.0, side_sem=None):
            self.name, self.buf, self.sem, self.side_sem = name, buf, sem, side_sem
            k = buf.shape[1]
            self.side = int(k * share) // 16 * 16 if cols > 1 and levels > 1 else 0
            self.k = k
            self.have = set()

        def piece(self, s, lo, hi):
            return self.buf.at[s] if (lo, hi) == (0, self.k) else self.buf.at[s, pl.ds(lo, hi - lo), :]

        def go(self, cond, s, lo, hi, sem, dev_sp):
            ref = self.piece(s, lo, hi)
            send(cond, ref, ref, sem.at[s], (dev_sp, t))

        def across(self, cond, s, lo=0):
            if lo == self.k:
                return
            for d in range(1, cols):
                self.go(cond, s, lo, self.k, self.sem, z * cols + (x + d) % cols)

        def begin_z(self):
            self.go(up, me, 0, self.k, self.sem, me + cols)
            self.go(down, me, 0, self.k, self.sem, me - cols)

        def begin_x(self):
            self.across(None, me)

        def forward(self, h):
            with jax.named_scope(f"f{self.name}{h}"):
                for level, there, on, to in at_distance(h):
                    s = level * cols + x
                    arrived(there, self.buf.at[s], self.sem.at[s])
                    self.go(both(there, on), s, 0, self.k, self.sem, to)
                    self.across(there, s, self.side if h == 1 else 0)

        def peers(self, level):
            return [level * cols + (x + cols - d) % cols for d in range(1, cols)]

        def forward_side(self):
            if not self.side:
                return
            self.take(0)
            sem = self.sem if self.side == self.k else self.side_sem
            for s in self.peers(z):
                self.go(up, s, 0, self.side, sem, me + cols)
                self.go(down, s, 0, self.side, sem, me - cols)

        def take(self, h):
            if h in self.have:
                return
            self.have.add(h)
            with jax.named_scope(f"t{self.name}{h}"):
                for level, there, _, _ in at_distance(h):
                    for s in self.peers(level):
                        if h == 1 and self.side and self.side < self.k:
                            arrived(there, self.piece(s, 0, self.side), self.side_sem.at[s])
                            arrived(there, self.piece(s, self.side, self.k), self.sem.at[s])
                        else:
                            arrived(there, self.buf.at[s], self.sem.at[s])

    spread_q = Spread("q", wq, sem_q)
    spread_kv = Spread("k", wkv, sem_kv)
    spread_p = Spread("p", wp, sem_p, 1.0)
    spread_a = Spread("a", wa, sem_a, 1.0)
    spread_b = Spread("b", wb, sem_b, 0.5, sem_b_side)
    for copy in locals_[:n_in]:
        copy.wait()
    for spread in (spread_q, spread_kv, spread_p):
        spread.begin_z()
        spread.begin_x()
    locals_[n_in].wait()

    mine = pl.ds(pl.multiple_of(t * rows, rows), rows)
    wide = tokv[...].astype(F32)
    inverse = lax.rsqrt(jnp.mean(wide * wide, axis=1, keepdims=True) + EPS)
    piece = xs.shape[2]
    for i in range(n_sp):
        span = slice(i * piece, (i + 1) * piece)
        xs[i, mine, :] = (tokv[:, span].astype(F32) * inverse * gain[:, span]).astype(BF16)

    def rows_of(device):
        return xs.at[:, pl.ds(pl.multiple_of(device * rows, rows), rows), :]

    for d in range(1, chips):
        send(None, rows_of(t), rows_of(t), sem_tok.at[t], (me, (y + d) % chips * CORES + c))
    send(None, rows_of(t), rows_of(t), sem_tok.at[t], (me, partner))

    def chip_rows(chip):
        return pl.ds(pl.multiple_of(chip * per, per), per)

    near = [y]
    far = [(y + d) % chips for d in range(1, chips)]

    def project(spread, at, h, which):
        spread.take(h)
        w = spread.buf.shape[2]
        with jax.named_scope(f"m{spread.name}{h}"):
            for level, there, _, _ in at_distance(h):

                def run(level=level):
                    for chip in which:
                        r = chip_rows(chip)
                        value = None
                        for i in range(cols):
                            s = level * cols + i
                            part = jnp.dot(
                                xs[s, r, :], spread.buf[s], preferred_element_type=F32
                            )
                            value = part if value is None else value + part
                        if h == 0:
                            acc[r, at : at + w] = value
                        else:
                            acc[r, at : at + w] += value

                when(there, run)

    def project_q(h, which):
        project(spread_q, 0, h, which)

    def project_kv(h, which):
        project(spread_kv, qw, h, which)

    def project_p(h, which):
        project(spread_p, channel0, h, which)

    arrived(None, rows_of(partner), sem_tok.at[partner])
    for copy in locals_[n_in + 1 :]:
        copy.wait()

    def gather_tokens():
        with jax.named_scope("tokf"):
            for d in range(1, chips):
                at = (y + chips - d) % chips * CORES + c
                arrived(None, rows_of(at), sem_tok.at[at])
                send(None, rows_of(at), rows_of(at), sem_tok.at[at], (me, partner))

    def take_tokens():
        with jax.named_scope("tokt"):
            for d in range(1, chips):
                at = (y + chips - d) % chips * CORES + (1 - c)
                arrived(None, rows_of(at), sem_tok.at[at])

    last = levels - 1
    for h in range(1, last):
        spread_q.forward(h)
        if h > 1:
            project_p(h - 2, near)
        spread_kv.forward(h)
        project_q(h - 1, near)
        spread_p.forward(h)
        project_kv(h - 1, near)
    spread_p.forward_side()
    spread_a.begin_z()
    gather_tokens()
    done = max(0, last - 1)
    if last:
        spread_q.forward(last)
    take_tokens()
    for h in range(done):
        project_q(h, far)
        project_kv(h, far)
    for h in range(max(0, last - 2)):
        project_p(h, far)
    if last:
        spread_kv.forward(last)
    for h in range(done, last):
        project_q(h, near + far)
        project_kv(h, near + far)
    if last:
        spread_p.forward(last)
    for h in range(max(0, last - 2), last):
        if h != 1:
            project_p(h, near + far)
    project_q(last, far + near)
    project_kv(last, far + near)

    def settle(lo, hi):
        for chip in range(chips):
            r = slice(chip * per, (chip + 1) * per)
            ext[WINDOW + chip * per : WINDOW + (chip + 1) * per, lo:hi] = acc[r, lo:hi].astype(BF16)

    with jax.named_scope("settleq"):
        settle(0, channel0)

    def pass_on(cond, at, width, n, i):
        head = ext.at[pl.ds(WINDOW - n, n), pl.ds(at, width)]
        tail = ext.at[pl.ds(seq + WINDOW - n, n), pl.ds(at, width)]
        send(both(cond, later), tail, head, sem_halo.at[i], (me + 1, t))
        return head

    head_kv = pass_on(None, qw, kw + vw, WINDOW, 0)
    spread_a.begin_x()
    spread_b.begin_z()

    group_heads = qw // kw
    stacked = group_heads * WINDOW
    scale = HEAD_DIM ** (-0.5)

    def attend(n):
        q_rows = pl.ds(pl.multiple_of(n * WINDOW + WINDOW, WINDOW), WINDOW)
        k_rows = pl.ds(pl.multiple_of(n * WINDOW, WINDOW), 2 * WINDOW)
        queries = ext[q_rows, :qw]
        keys = ext[k_rows, qw : qw + kw]
        values = ext[k_rows, qw + kw : channel0]
        row = lax.broadcasted_iota(jnp.int32, (stacked, 2 * WINDOW), 0)
        q_index = row % WINDOW
        k_index = lax.broadcasted_iota(jnp.int32, (stacked, 2 * WINDOW), 1)
        lowest = jnp.where(me * blocks + n == 0, WINDOW, 0)
        allowed = (k_index > q_index) & (k_index <= q_index + WINDOW) & (k_index >= lowest)
        which = lax.broadcasted_iota(jnp.int32, (stacked, 1), 0) // WINDOW
        done = []
        for j in range(kw // HEAD_DIM):
            part = slice(j * HEAD_DIM, (j + 1) * HEAD_DIM)
            first = j * group_heads
            q = jnp.concatenate(
                [
                    queries[:, (first + g) * HEAD_DIM : (first + g + 1) * HEAD_DIM]
                    for g in range(group_heads)
                ],
                axis=0,
            )
            scores = (
                lax.dot_general(
                    q, keys[:, part], (((1,), (1,)), ((), ())), preferred_element_type=F32
                )
                * scale
            )
            scores = jnp.where(allowed, scores, -jnp.inf)
            sinks = jnp.full((stacked, 1), sink[first], F32)
            for g in range(1, group_heads):
                sinks = jnp.where(which == g, sink[first + g], sinks)
            peak = jnp.maximum(jnp.max(scores, axis=1, keepdims=True), sinks)
            expo = jnp.exp(scores - peak)
            denom = jnp.sum(expo, axis=1, keepdims=True) + jnp.exp(sinks - peak)
            probs = (expo * (1.0 / denom)).astype(BF16)
            got = jnp.dot(probs, values[:, part], preferred_element_type=F32)
            done += [got[g * WINDOW : (g + 1) * WINDOW] for g in range(group_heads)]
        to = pl.ds(pl.multiple_of(n * WINDOW, WINDOW), WINDOW)
        mix[to, :qw] = jnp.concatenate(done, axis=1).astype(BF16)

    group = t * pw // POOL_CH
    whole_prefix = group == POOL_GROUPS - 1

    third = max(2, 2 * blocks // 3)
    with jax.named_scope("att1"):
        pl.loop(1, third)(attend)
    if last:
        spread_a.forward(1)
    if last >= 1:
        for h in sorted({1, last}):
            project_p(h, far + near)
    with jax.named_scope("settlep"):
        settle(channel0, ext.shape[1])
    heads_pool = []
    for g, reach in enumerate(SHORT_REACHES + (WINDOW,)):
        n = -(-(reach - 1) // 16) * 16
        heads_pool.append((group == g, pass_on(group == g, channel0, pw, n, 1)))
    total = jnp.sum(ext[WINDOW:, channel0:].astype(F32), axis=0, keepdims=True)
    tot[me] = jnp.broadcast_to(total, tot.shape[1:])
    for d in range(1, n_sp):
        send(
            both(whole_prefix, me + d < n_sp), tot.at[me], tot.at[me], sem_tot.at[me],
            (me + d, t),
        )
    spread_b.begin_x()
    if last:
        spread_b.forward(1)
    with jax.named_scope("att2"):
        pl.loop(third, blocks)(attend)
    with jax.named_scope("halokv"):
        arrived(earlier, head_kv, sem_halo.at[0])
    with jax.named_scope("att0"):
        attend(0)
    if last >= 2:
        spread_a.forward(2)
    with jax.named_scope("halopool"):
        for cond, head in heads_pool:
            arrived(both(cond, earlier), head, sem_halo.at[1])
    carry[...] = jnp.zeros(carry.shape, F32)
    for d in range(1, n_sp):

        def add(d=d):
            arrived(None, tot.at[me - d], sem_tot.at[me - d])
            carry[...] += tot[me - d]

        when(both(whole_prefix, me - d >= 0), add)

    reach = jnp.where(
        group == 0, SHORT_REACHES[0], jnp.where(group == 1, SHORT_REACHES[1], WINDOW)
    )
    reach = jnp.where(whole_prefix, n_sp * seq, reach)
    lowest = jnp.where(whole_prefix, WINDOW, 0)
    scope = jax.named_scope("pool")
    scope.__enter__()

    @pl.loop(0, blocks)
    def _(n):
        q_index = lax.broadcasted_iota(jnp.int32, (WINDOW, 2 * WINDOW), 0)
        k_index = lax.broadcasted_iota(jnp.int32, (WINDOW, 2 * WINDOW), 1)
        distance = q_index + WINDOW - k_index
        band = (distance >= 0) & (distance < reach) & (k_index >= lowest)
        band = jnp.where(band, 1.0, 0.0).astype(BF16)
        k_rows = pl.ds(pl.multiple_of(n * WINDOW, WINDOW), 2 * WINDOW)
        both_blocks = ext[k_rows, channel0:]
        sums = jnp.dot(band, both_blocks, preferred_element_type=F32) + carry[0:1, :]
        position = me * seq + n * WINDOW + lax.broadcasted_iota(jnp.int32, (WINDOW, 1), 0)
        counted = jnp.minimum(position + 1, reach).astype(F32)
        mixed = (sums / counted - both_blocks[WINDOW:].astype(F32)) * pgain[...]
        mix[pl.ds(pl.multiple_of(n * WINDOW, WINDOW), WINDOW), qw:] = mixed.astype(BF16)
        carry[...] = jnp.where(
            whole_prefix, jnp.broadcast_to(sums[WINDOW - 1 :], carry.shape), 0.0
        )

    scope.__exit__(None, None, None)

    def product(s, chip, core):
        r = pl.ds(pl.multiple_of((chip * CORES + core) * rows, rows), rows)
        return jnp.dot(mix[r, :qw], wa[s], preferred_element_type=F32) + jnp.dot(
            mix[r, qw:], wb[s], preferred_element_type=F32
        )

    def multiply(tag, cond, s):
        def give():
            for i, chip in enumerate(far):
                dfar[s, i] = product(s, chip, 1 - c).astype(BF16)

        def give_near():
            dnear[s] = product(s, y, 1 - c).astype(BF16)

        def keep():
            for i, chip in enumerate(far):
                ofar[s, i] = product(s, chip, c)

        def keep_near():
            onear[s] = product(s, y, c)

        with jax.named_scope(f"mul{tag}"):
            if chips > 1:
                when(cond, give)
                send(cond, dfar.at[s], rfar.at[s], sem_far.at[s], (me, partner))
                when(cond, keep)
            when(cond, give_near)
            send(cond, dnear.at[s], rnear.at[s], sem_near.at[s], (me, partner))
            when(cond, keep_near)
        if chips == 1:
            return
        with jax.named_scope(f"fin{tag}"):
            arrived(cond, rfar.at[s], sem_far.at[s])

            def pack():
                for i in range(chips - 1):
                    ysend[s, i] = (ofar[s, i] + rfar[s, i].astype(F32)).astype(BF16)

            when(cond, pack)
            for i, chip in enumerate(far):
                send(
                    cond, ysend.at[s, i], yrecv.at[s, i], sem_y.at[s, i], (me, chip * CORES + c)
                )

    order = []

    def column(h):
        for i, (level, there, _, _) in enumerate(at_distance(h)):
            order.append((there, level * cols + x))
            multiply(f"c{h}_{i}", there, level * cols + x)

    def others(h):
        spread_a.take(h)
        spread_b.take(h)
        for i, (level, there, _, _) in enumerate(at_distance(h)):
            for s in spread_a.peers(level):
                order.append((there, s))
                multiply(f"o{h}_{i}", there, s)

    column(0)
    if last >= 2:
        spread_b.forward(2)
    spread_a.forward_side()
    spread_b.forward_side()
    if last:
        column(1)
    if last >= 3:
        spread_a.forward(3)
    others(0)
    if last >= 3:
        spread_b.forward(3)
    for h in range(2, last):
        column(h)
        others(h)
    if last > 1:
        column(last)
    if last:
        others(1)
    if last > 1:
        others(last)

    with jax.named_scope("final"):
        w = wa.shape[2]
        for cond, s in order:

            def end(s=s):
                arrived(None, rnear.at[s], sem_near.at[s])
                value = onear[s] + rnear[s].astype(F32)
                for i in range(chips - 1):
                    arrived(None, yrecv.at[s, i], sem_y.at[s, i])
                    value += yrecv[s, i].astype(F32)
                out[:, pl.ds(pl.multiple_of(s * w, w), w)] = value.astype(BF16)

            when(cond, end)

    with jax.named_scope("wsend"):
        for item in slots:
            if item is not None:
                when(item[0], item[1].wait_send)


def local(
    n_sp, n_tp, tokens_in, norm_gain, query_weight, key_weight, value_weight, pool_weight,
    sink_logit, pool_gain, attention_out_weight, pool_out_weight,
):
    rows, depth = tokens_in.shape
    seq = rows * n_tp
    ins = [query_weight, key_weight, value_weight, pool_weight]
    outs = [attention_out_weight, pool_out_weight]
    widths = tuple(w.shape[1] for w in ins)
    if widths[1] % 128:
        ins = [ins[0], jnp.concatenate(ins[1:3], axis=1), ins[3]]
    cols = math.gcd(n_sp, max(1, n_tp // CORES))
    chips = n_tp // CORES
    k_in, out_cols = ins[0].shape[0], outs[0].shape[1]
    width, others = sum(widths), max(1, chips - 1)
    qw, kw, vw, pw = widths
    vmem = pl.BlockSpec(memory_space=pltpu.VMEM)
    hbm = pl.BlockSpec(memory_space=pl.ANY)
    dma = pltpu.SemaphoreType.DMA
    return pl.pallas_call(
        functools.partial(kernel, n_sp, n_tp, cols, len(ins), len(outs), widths),
        out_shape=pltpu.VMEM((rows, depth), BF16),
        in_specs=[hbm, vmem, pl.BlockSpec(memory_space=pltpu.SMEM), vmem]
        + [hbm] * (len(ins) + len(outs)),
        out_specs=vmem,
        scratch_shapes=[
            pltpu.VMEM((rows, depth), BF16),
            pltpu.VMEM((n_sp, seq, depth // n_sp), BF16),
            pltpu.VMEM((n_sp, k_in, qw), BF16),
            pltpu.VMEM((n_sp, k_in, kw + vw), BF16),
            pltpu.VMEM((n_sp, k_in, pw), BF16),
            pltpu.VMEM((n_sp, outs[0].shape[0], out_cols), BF16),
            pltpu.VMEM((n_sp, outs[1].shape[0], out_cols), BF16),
            pltpu.VMEM((seq, width), F32),
            pltpu.VMEM((seq + WINDOW, width), BF16),
            pltpu.VMEM((seq, qw + pw), BF16),
            pltpu.VMEM((n_sp, 8, pw), F32),
            pltpu.VMEM((8, pw), F32),
            pltpu.VMEM((n_sp, others, rows, out_cols), BF16),
            pltpu.VMEM((n_sp, others, rows, out_cols), BF16),
            pltpu.VMEM((n_sp, rows, out_cols), BF16),
            pltpu.VMEM((n_sp, rows, out_cols), BF16),
            pltpu.VMEM((n_sp, others, rows, out_cols), BF16),
            pltpu.VMEM((n_sp, others, rows, out_cols), BF16),
            pltpu.VMEM((n_sp, others, rows, out_cols), F32),
            pltpu.VMEM((n_sp, rows, out_cols), F32),
            dma((len(ins) + len(outs) + 1,)),
            dma((SEND_SLOTS,)),
            dma((n_sp,)),
            dma((n_sp,)),
            dma((n_sp,)),
            dma((n_sp,)),
            dma((n_sp,)),
            dma((n_sp,)),
            dma((n_tp,)),
            dma((2,)),
            dma((n_sp,)),
            dma((n_sp,)),
            dma((n_sp,)),
            dma((n_sp, others)),
        ],
        compiler_params=pltpu.CompilerParams(
            collective_id=0, has_side_effects=True, vmem_limit_bytes=58 << 20
        ),
    )(
        tokens_in, norm_gain.reshape(1, -1), sink_logit, pool_gain.reshape(1, -1), *ins, *outs
    )


def solution(mesh):
    in_specs = (
        P(("sp", "tp"), None), P(), P("sp", "tp"), P("sp", "tp"), P("sp", "tp"), P("sp", "tp"),
        P("tp"), P("tp"), P("tp", "sp"), P("tp", "sp"),
    )
    out_specs = P(("sp", "tp"), None)
    return jax.shard_map(
        functools.partial(local, mesh.shape["sp"], mesh.shape["tp"]),
        mesh=mesh, in_specs=in_specs, out_specs=out_specs, check_vma=False,
    )
```

time: 85.8 us -> 69.5 us (0.81)
  the two profiles are of different devices: /device:TPU:0 before, /device:TPU:27 now
where the time goes in v1:
time: 69.5 us; the launch traced here: 69.3 us
  Pallas kernels  68.4 us (98%)
  local copies, waits for them, and re-layouts  0.88 us (1%)
    pallas_call x1, Pallas kernels, local(): pl.pallas_call(functools.partial(kernel, n_sp, n_tp, cols, len(ins), len(...  68.4 us

profile of v1, /device:TPU:27, one launch (start us, length us, event | category | flops | bytes accessed | tf_op | source)
XLA Modules:
  0.0 69.3 jit_solution(5591578261566015463)
XLA Ops:
  0.0 68.4 %shard_map.100 = bf16[192,2048]{1,0:T(8,128)(2,1)S(1)} custom-call(bf16[192,2048]{1,0:T(8,128)(2,1)} %refs_0_.1, f32[1,2048]{1,0:T(1,128)} %bitcast.2, f32[4]{0:T(128)} %refs_2_.1, f32[1,256]{1,0:T(1,128)} %bitcast.3, bf16[256,256]{1,0:T(8,128)(2,1)} %refs_4_.1, bf16[256,128]{1,0:T(8,128)(2,1)} %refs_5_.1, bf16[256,128]{1,0:T(8,128)(2,1)} %refs_6_.1, ...), custom_call_target="tpu_custom_call" | custom-call | tf_op jit(solution)/shard_map/pallas_call | solution.py:572
  68.4 0.9 %copy.12 = bf16[192,2048]{1,0:T(8,128)(2,1)} copy(bf16[192,2048]{1,0:T(8,128)(2,1)S(1)} %shard_map.100) | data formatting | bytes 1572864

commit v2 on v1

--- a/solution.py
+++ b/solution.py
@@ -15,7 +15,7 @@
 EPS = 1e-06
 SHORT_REACHES = (8, 32)
 CORES = 2
-SEND_SLOTS = 32
+SEND_SLOTS = 40
 MESH = pl.DeviceIdType.MESH
 F32 = jnp.float32
 BF16 = jnp.bfloat16
@@ -33,13 +33,13 @@
 
 
 def kernel(n_sp, n_tp, cols, n_in, n_out, widths, *refs):
-    tok, gain, sink, pgain = refs[:4]
+    tok, gain_in, sink_in, pgain_in = refs[:4]
     win_refs = refs[4 : 4 + n_in]
     wout_refs = refs[4 + n_in : 4 + n_in + n_out]
     (
-        out, tokv, xs, wq, wkv, wp, wa, wb, acc, ext, mix, tot, carry, dfar, rfar, dnear, rnear,
-        ysend, yrecv, ofar, onear,
-        local_sem, send_sem, sem_q, sem_kv, sem_p, sem_a, sem_b, sem_b_side,
+        out, tokv, xs, wq, wkv, wp, wa, wb, acc, ext, mix, tot, carry, given, dfar, rfar, dnear, rnear,
+        ysend, yrecv, ofar, onear, gain, pgain, sink,
+        local_sem, send_sem, once_sem, sem_q, sem_kv, sem_p, sem_a, sem_b, sem_a_side,
         sem_tok, sem_halo, sem_tot, sem_far, sem_near, sem_y,
     ) = refs[4 + n_in + n_out :]
     qw, kw, vw, pw = widths
@@ -55,24 +55,10 @@
     partner = y * CORES + (1 - c)
     up, down = z + 1 < levels, z > 0
     later, earlier = me + 1 < n_sp, me > 0
-
-    locals_ = []
-
-    def fetch(src, dst):
-        copy = pltpu.make_async_copy(src, dst, local_sem.at[len(locals_)])
-        copy.start()
-        locals_.append(copy)
-
-    fetch(win_refs[0], wq.at[me])
-    at = 0
-    for ref in win_refs[1:-1]:
-        w = ref.shape[1]
-        fetch(ref, wkv.at[me, :, pl.ds(at, w)])
-        at += w
-    fetch(win_refs[-1], wp.at[me])
-    fetch(tok, tokv)
-    fetch(wout_refs[0], wa.at[me])
-    fetch(wout_refs[1], wb.at[me])
+    last = levels - 1
+    at_end = jnp.logical_or(z == 0, z == last)
+    inner = jnp.logical_not(at_end)
+
     ext[:WINDOW, qw:] = jnp.zeros((WINDOW, ext.shape[1] - qw), BF16)
 
     barrier = pltpu.get_barrier_semaphore()
@@ -100,6 +86,26 @@
     expected = cols - 1 + n_tp - 1 + jnp.where(up, 1, 0) + jnp.where(down, 1, 0)
     if greet_diagonal:
         expected = expected + jnp.where(next_row, 1, 0) + jnp.where(last_row, 1, 0)
+    locals_ = []
+
+    def fetch(src, dst):
+        copy = pltpu.make_async_copy(src, dst, local_sem.at[len(locals_)])
+        copy.start()
+        locals_.append(copy)
+
+    fetch(win_refs[0], wq.at[me])
+    at = 0
+    for ref in win_refs[1:-1]:
+        w = ref.shape[1]
+        fetch(ref, wkv.at[me, :, pl.ds(at, w)])
+        at += w
+    fetch(win_refs[-1], wp.at[me])
+    fetch(tok, tokv)
+    fetch(gain_in, gain)
+    fetch(wout_refs[0], wa.at[me])
+    fetch(wout_refs[1], wb.at[me])
+    fetch(pgain_in, pgain)
+    fetch(sink_in, sink)
     with jax.named_scope("barrier"):
         pl.semaphore_wait(barrier, expected)
 
@@ -118,6 +124,16 @@
         when(cond, copy.start)
         slots[slot] = (cond, copy)
 
+    fixed = []
+
+    def send_once(cond, src, dst, sem, recv, dev):
+        copy = pltpu.make_async_remote_copy(
+            src_ref=src, dst_ref=dst, send_sem=sem, recv_sem=recv, device_id=dev,
+            device_id_type=MESH,
+        )
+        when(cond, copy.start)
+        fixed.append((cond, copy))
+
     def arrived(cond, dst, recv):
         copy = pltpu.make_async_remote_copy(
             src_ref=dst, dst_ref=dst, send_sem=send_sem.at[0], recv_sem=recv,
@@ -134,15 +150,23 @@
         )
 
     class Spread:
-        def __init__(self, name, buf, sem, share=0.0, side_sem=None):
+        def __init__(
+            self, name, buf, sem, share=0.0, side_sem=None, ends=False, next_too=False
+        ):
             self.name, self.buf, self.sem, self.side_sem = name, buf, sem, side_sem
             k = buf.shape[1]
             self.side = int(k * share) // 16 * 16 if cols > 1 and levels > 1 else 0
-            self.k = k
-            self.have = set()
+            self.k, self.ends, self.next_too = k, ends, next_too and cols > 1 and last > 1
+            self.have, self.have_at_ends = set(), set()
 
         def piece(self, s, lo, hi):
             return self.buf.at[s] if (lo, hi) == (0, self.k) else self.buf.at[s, pl.ds(lo, hi - lo), :]
+
+        def side_at(self, h):
+            return self.side if h == (last if self.ends else 1) else 0
+
+        def side_sems(self):
+            return self.sem if self.side == self.k else self.side_sem
 
         def go(self, cond, s, lo, hi, sem, dev_sp):
             ref = self.piece(s, lo, hi)
@@ -154,20 +178,25 @@
             for d in range(1, cols):
                 self.go(cond, s, lo, self.k, self.sem, z * cols + (x + d) % cols)
 
-        def begin_z(self):
-            self.go(up, me, 0, self.k, self.sem, me + cols)
+        def begin_up(self, cond=None):
+            self.go(both(up, cond), me, 0, self.k, self.sem, me + cols)
+
+        def begin_down(self):
             self.go(down, me, 0, self.k, self.sem, me - cols)
 
-        def begin_x(self):
-            self.across(None, me)
-
-        def forward(self, h):
+        def begin_x(self, cond=None):
+            self.across(cond, me)
+
+        def forward(self, h, cond=None):
             with jax.named_scope(f"f{self.name}{h}"):
                 for level, there, on, to in at_distance(h):
+                    there = both(there, cond)
                     s = level * cols + x
                     arrived(there, self.buf.at[s], self.sem.at[s])
                     self.go(both(there, on), s, 0, self.k, self.sem, to)
-                    self.across(there, s, self.side if h == 1 else 0)
+                    if self.next_too and h == 1:
+                        there = both(there, jnp.logical_and(level != 0, level != last))
+                    self.across(there, s, self.side_at(h))
 
         def peers(self, level):
             return [level * cols + (x + cols - d) % cols for d in range(1, cols)]
@@ -175,36 +204,55 @@
         def forward_side(self):
             if not self.side:
                 return
-            self.take(0)
-            sem = self.sem if self.side == self.k else self.side_sem
+            if not self.ends:
+                self.take(0)
+            sem = self.side_sems()
             for s in self.peers(z):
-                self.go(up, s, 0, self.side, sem, me + cols)
-                self.go(down, s, 0, self.side, sem, me - cols)
-
-        def take(self, h):
-            if h in self.have:
+                if not self.ends:
+                    self.go(up, s, 0, self.side, sem, me + cols)
+                    self.go(down, s, 0, self.side, sem, me - cols)
+                    continue
+                self.go(at_end, s, 0, self.side, sem, (last - z) * cols + x)
+
+        def forward_next(self):
+            if not self.next_too:
                 return
-            self.have.add(h)
+            self.take(0, at_end)
+            for s in self.peers(z):
+                self.go(z == 0, s, 0, self.k, self.sem, me + cols)
+                self.go(z == last, s, 0, self.k, self.sem, me - cols)
+
+        def take(self, h, cond=None):
+            if h in self.have or (h in self.have_at_ends and cond is at_end):
+                return
+            if cond is at_end:
+                self.have_at_ends.add(h)
+            else:
+                self.have.add(h)
+                cond = inner if h in self.have_at_ends else cond
+            side = self.side_at(h)
             with jax.named_scope(f"t{self.name}{h}"):
                 for level, there, _, _ in at_distance(h):
+                    there = both(there, cond)
                     for s in self.peers(level):
-                        if h == 1 and self.side and self.side < self.k:
-                            arrived(there, self.piece(s, 0, self.side), self.side_sem.at[s])
-                            arrived(there, self.piece(s, self.side, self.k), self.sem.at[s])
-                        else:
-                            arrived(there, self.buf.at[s], self.sem.at[s])
-
-    spread_q = Spread("q", wq, sem_q)
-    spread_kv = Spread("k", wkv, sem_kv)
+                        if side:
+                            arrived(there, self.piece(s, 0, side), self.side_sems().at[s])
+                        if side < self.k:
+                            arrived(there, self.piece(s, side, self.k), self.sem.at[s])
+
+    spread_q = Spread("q", wq, sem_q, next_too=True)
+    spread_kv = Spread("k", wkv, sem_kv, next_too=True)
     spread_p = Spread("p", wp, sem_p, 1.0)
-    spread_a = Spread("a", wa, sem_a, 1.0)
-    spread_b = Spread("b", wb, sem_b, 0.5, sem_b_side)
+    spread_a = Spread("a", wa, sem_a, 0.5, sem_a_side, True, True)
+    spread_b = Spread("b", wb, sem_b, 1.0, None, True, True)
     for copy in locals_[:n_in]:
         copy.wait()
     for spread in (spread_q, spread_kv, spread_p):
-        spread.begin_z()
+        spread.begin_up()
+        spread.begin_down()
         spread.begin_x()
     locals_[n_in].wait()
+    locals_[n_in + 1].wait()
 
     mine = pl.ds(pl.multiple_of(t * rows, rows), rows)
     wide = tokv[...].astype(F32)
@@ -260,7 +308,7 @@
         project(spread_p, channel0, h, which)
 
     arrived(None, rows_of(partner), sem_tok.at[partner])
-    for copy in locals_[n_in + 1 :]:
+    for copy in locals_[n_in + 2 :]:
         copy.wait()
 
     def gather_tokens():
@@ -276,17 +324,23 @@
                 at = (y + chips - d) % chips * CORES + (1 - c)
                 arrived(None, rows_of(at), sem_tok.at[at])
 
-    last = levels - 1
     for h in range(1, last):
         spread_q.forward(h)
         if h > 1:
             project_p(h - 2, near)
         spread_kv.forward(h)
+        if h == 1:
+            spread_q.forward_next()
         project_q(h - 1, near)
         spread_p.forward(h)
+        if h == 1:
+            spread_kv.forward_next()
         project_kv(h - 1, near)
     spread_p.forward_side()
-    spread_a.begin_z()
+    spread_a.begin_down()
+    spread_a.begin_up()
+    spread_b.begin_down()
+    spread_b.begin_up(at_end)
     gather_tokens()
     done = max(0, last - 1)
     if last:
@@ -308,6 +362,8 @@
         if h != 1:
             project_p(h, near + far)
     project_q(last, far + near)
+    if last:
+        project_p(1, far + near)
     project_kv(last, far + near)
 
     def settle(lo, hi):
@@ -321,12 +377,52 @@
     def pass_on(cond, at, width, n, i):
         head = ext.at[pl.ds(WINDOW - n, n), pl.ds(at, width)]
         tail = ext.at[pl.ds(seq + WINDOW - n, n), pl.ds(at, width)]
-        send(both(cond, later), tail, head, sem_halo.at[i], (me + 1, t))
+        send_once(
+            both(cond, later), tail, head, once_sem.at[i], sem_halo.at[i], (me + 1, t)
+        )
         return head
 
     head_kv = pass_on(None, qw, kw + vw, WINDOW, 0)
+
+    group = t * pw // POOL_CH
+    whole_prefix = group == POOL_GROUPS - 1
+    halos = [
+        (group == g, -(-(reach - 1) // 16) * 16)
+        for g, reach in enumerate(SHORT_REACHES + (WINDOW,))
+    ]
+
+    def finish_pool_rows(cond):
+        def run():
+            with jax.named_scope("settlep"):
+                settle(channel0, ext.shape[1])
+                for n in range(blocks):
+                    r = slice(WINDOW + n * WINDOW, 2 * WINDOW + n * WINDOW)
+                    total = jnp.sum(ext[r, channel0:].astype(F32), axis=0, keepdims=True)
+                    if n + 1 < blocks:
+                        carry[n + 1] = jnp.broadcast_to(
+                            total if n == 0 else carry[n, 0:1, :] + total, carry.shape[1:]
+                        )
+                    else:
+                        tot[me] = jnp.broadcast_to(
+                            total if n == 0 else carry[n, 0:1, :] + total, tot.shape[1:]
+                        )
+                carry[0] = jnp.zeros(carry.shape[1:], F32)
+
+        when(cond, run)
+        for is_group, n in halos:
+            pass_on(both(is_group, cond), channel0, pw, n, 1)
+        for d in range(1, n_sp):
+            send_once(
+                both(both(whole_prefix, cond), me + d < n_sp), tot.at[me], tot.at[me],
+                once_sem.at[1 + d], sem_tot.at[me], (me + d, t),
+            )
+
+    finish_pool_rows(inner)
     spread_a.begin_x()
-    spread_b.begin_z()
+    spread_b.begin_x(inner)
+    spread_b.begin_up(inner)
+    if last:
+        spread_a.forward(1, inner)
 
     group_heads = qw // kw
     stacked = group_heads * WINDOW
@@ -374,80 +470,80 @@
         to = pl.ds(pl.multiple_of(n * WINDOW, WINDOW), WINDOW)
         mix[to, :qw] = jnp.concatenate(done, axis=1).astype(BF16)
 
-    group = t * pw // POOL_CH
-    whole_prefix = group == POOL_GROUPS - 1
-
-    third = max(2, 2 * blocks // 3)
-    with jax.named_scope("att1"):
-        pl.loop(1, third)(attend)
-    if last:
-        spread_a.forward(1)
-    if last >= 1:
-        for h in sorted({1, last}):
-            project_p(h, far + near)
-    with jax.named_scope("settlep"):
-        settle(channel0, ext.shape[1])
-    heads_pool = []
-    for g, reach in enumerate(SHORT_REACHES + (WINDOW,)):
-        n = -(-(reach - 1) // 16) * 16
-        heads_pool.append((group == g, pass_on(group == g, channel0, pw, n, 1)))
-    total = jnp.sum(ext[WINDOW:, channel0:].astype(F32), axis=0, keepdims=True)
-    tot[me] = jnp.broadcast_to(total, tot.shape[1:])
-    for d in range(1, n_sp):
-        send(
-            both(whole_prefix, me + d < n_sp), tot.at[me], tot.at[me], sem_tot.at[me],
-            (me + d, t),
-        )
-    spread_b.begin_x()
-    if last:
-        spread_b.forward(1)
-    with jax.named_scope("att2"):
-        pl.loop(third, blocks)(attend)
-    with jax.named_scope("halokv"):
-        arrived(earlier, head_kv, sem_halo.at[0])
-    with jax.named_scope("att0"):
-        attend(0)
-    if last >= 2:
-        spread_a.forward(2)
-    with jax.named_scope("halopool"):
-        for cond, head in heads_pool:
-            arrived(both(cond, earlier), head, sem_halo.at[1])
-    carry[...] = jnp.zeros(carry.shape, F32)
-    for d in range(1, n_sp):
-
-        def add(d=d):
-            arrived(None, tot.at[me - d], sem_tot.at[me - d])
-            carry[...] += tot[me - d]
-
-        when(both(whole_prefix, me - d >= 0), add)
+    if per % WINDOW == 0:
+        span = per // WINDOW
+        far_blocks, near_blocks = [chip * span for chip in far], [y * span]
+    else:
+        span = blocks
+        far_blocks, near_blocks = [0], []
+
+    def attend_later_blocks(firsts):
+        with jax.named_scope("att"):
+            for first in firsts:
+                pl.loop(1, span)(lambda i, first=first: attend(first + i))
+
+    def attend_first_block(firsts):
+        with jax.named_scope("att0"):
+            for first in firsts:
+                cond = earlier if isinstance(first, int) else both(earlier, first == 0)
+                arrived(cond, head_kv, sem_halo.at[0])
+                attend(first)
 
     reach = jnp.where(
         group == 0, SHORT_REACHES[0], jnp.where(group == 1, SHORT_REACHES[1], WINDOW)
     )
     reach = jnp.where(whole_prefix, n_sp * seq, reach)
     lowest = jnp.where(whole_prefix, WINDOW, 0)
-    scope = jax.named_scope("pool")
-    scope.__enter__()
-
-    @pl.loop(0, blocks)
-    def _(n):
-        q_index = lax.broadcasted_iota(jnp.int32, (WINDOW, 2 * WINDOW), 0)
-        k_index = lax.broadcasted_iota(jnp.int32, (WINDOW, 2 * WINDOW), 1)
-        distance = q_index + WINDOW - k_index
-        band = (distance >= 0) & (distance < reach) & (k_index >= lowest)
-        band = jnp.where(band, 1.0, 0.0).astype(BF16)
-        k_rows = pl.ds(pl.multiple_of(n * WINDOW, WINDOW), 2 * WINDOW)
-        both_blocks = ext[k_rows, channel0:]
-        sums = jnp.dot(band, both_blocks, preferred_element_type=F32) + carry[0:1, :]
-        position = me * seq + n * WINDOW + lax.broadcasted_iota(jnp.int32, (WINDOW, 1), 0)
-        counted = jnp.minimum(position + 1, reach).astype(F32)
-        mixed = (sums / counted - both_blocks[WINDOW:].astype(F32)) * pgain[...]
-        mix[pl.ds(pl.multiple_of(n * WINDOW, WINDOW), WINDOW), qw:] = mixed.astype(BF16)
-        carry[...] = jnp.where(
-            whole_prefix, jnp.broadcast_to(sums[WINDOW - 1 :], carry.shape), 0.0
-        )
-
-    scope.__exit__(None, None, None)
+
+    def pool(firsts):
+        with jax.named_scope("pool"):
+            for first in firsts:
+
+                @pl.loop(0, span)
+                def _(i, first=first):
+                    n = first + i
+                    q_index = lax.broadcasted_iota(jnp.int32, (WINDOW, 2 * WINDOW), 0)
+                    k_index = lax.broadcasted_iota(jnp.int32, (WINDOW, 2 * WINDOW), 1)
+                    distance = q_index + WINDOW - k_index
+                    band = (distance >= 0) & (distance < reach) & (k_index >= lowest)
+                    band = jnp.where(band, 1.0, 0.0).astype(BF16)
+                    k_rows = pl.ds(pl.multiple_of(n * WINDOW, WINDOW), 2 * WINDOW)
+                    both_blocks = ext[k_rows, channel0:]
+                    before = jnp.where(whole_prefix, carry[n, 0:1, :] + given[0:1, :], 0.0)
+                    sums = jnp.dot(band, both_blocks, preferred_element_type=F32) + before
+                    position = (
+                        me * seq + n * WINDOW + lax.broadcasted_iota(jnp.int32, (WINDOW, 1), 0)
+                    )
+                    counted = jnp.minimum(position + 1, reach).astype(F32)
+                    mixed = (sums / counted - both_blocks[WINDOW:].astype(F32)) * pgain[...]
+                    to = pl.ds(pl.multiple_of(n * WINDOW, WINDOW), WINDOW)
+                    mix[to, qw:] = mixed.astype(BF16)
+
+    attend_later_blocks(far_blocks)
+    if last >= 2:
+        project_p(last, far + near)
+    finish_pool_rows(at_end)
+    spread_b.begin_x(at_end)
+    if last:
+        spread_a.forward(1, at_end)
+        spread_b.forward(1, inner)
+    attend_first_block(far_blocks)
+    if last:
+        spread_b.forward(1, at_end)
+    spread_a.forward_next()
+    with jax.named_scope("halopool"):
+        for cond, n in halos:
+            head = ext.at[pl.ds(WINDOW - n, n), pl.ds(channel0, pw)]
+            arrived(both(cond, earlier), head, sem_halo.at[1])
+        given[...] = jnp.zeros(given.shape, F32)
+        for d in range(1, n_sp):
+
+            def add(d=d):
+                arrived(None, tot.at[me - d], sem_tot.at[me - d])
+                given[...] += tot[me - d]
+
+            when(both(whole_prefix, me - d >= 0), add)
+    pool(far_blocks)
 
     def product(s, chip, core):
         r = pl.ds(pl.multiple_of((chip * CORES + core) * rows, rows), rows)
@@ -455,80 +551,124 @@
             mix[r, qw:], wb[s], preferred_element_type=F32
         )
 
-    def multiply(tag, cond, s):
-        def give():
-            for i, chip in enumerate(far):
-                dfar[s, i] = product(s, chip, 1 - c).astype(BF16)
-
-        def give_near():
-            dnear[s] = product(s, y, 1 - c).astype(BF16)
-
-        def keep():
-            for i, chip in enumerate(far):
-                ofar[s, i] = product(s, chip, c)
-
-        def keep_near():
-            onear[s] = product(s, y, c)
-
-        with jax.named_scope(f"mul{tag}"):
-            if chips > 1:
+    def column(h):
+        return [(there, level * cols + x) for level, there, _, _ in at_distance(h)]
+
+    def others(h):
+        return [
+            (there, s)
+            for level, there, _, _ in at_distance(h)
+            for s in spread_a.peers(level)
+        ]
+
+    def multiply_far(pieces):
+        for cond, s in pieces if chips > 1 else ():
+
+            def give(s=s):
+                for i, chip in enumerate(far):
+                    dfar[s, i] = product(s, chip, 1 - c).astype(BF16)
+
+            def keep(s=s):
+                for i, chip in enumerate(far):
+                    ofar[s, i] = product(s, chip, c)
+
+            with jax.named_scope("mulf"):
                 when(cond, give)
                 send(cond, dfar.at[s], rfar.at[s], sem_far.at[s], (me, partner))
                 when(cond, keep)
-            when(cond, give_near)
-            send(cond, dnear.at[s], rnear.at[s], sem_near.at[s], (me, partner))
-            when(cond, keep_near)
-        if chips == 1:
-            return
-        with jax.named_scope(f"fin{tag}"):
-            arrived(cond, rfar.at[s], sem_far.at[s])
-
-            def pack():
+
+    def multiply_near(pieces):
+        for cond, s in pieces:
+
+            def give_near(s=s):
+                dnear[s] = product(s, y, 1 - c).astype(BF16)
+
+            def keep_near(s=s):
+                onear[s] = product(s, y, c)
+
+            with jax.named_scope("muln"):
+                when(cond, give_near)
+                send(cond, dnear.at[s], rnear.at[s], sem_near.at[s], (me, partner))
+                when(cond, keep_near)
+
+    def finish(pieces):
+        for cond, s in pieces if chips > 1 else ():
+
+            def pack(s=s):
                 for i in range(chips - 1):
                     ysend[s, i] = (ofar[s, i] + rfar[s, i].astype(F32)).astype(BF16)
 
-            when(cond, pack)
-            for i, chip in enumerate(far):
-                send(
-                    cond, ysend.at[s, i], yrecv.at[s, i], sem_y.at[s, i], (me, chip * CORES + c)
-                )
-
-    order = []
-
-    def column(h):
-        for i, (level, there, _, _) in enumerate(at_distance(h)):
-            order.append((there, level * cols + x))
-            multiply(f"c{h}_{i}", there, level * cols + x)
-
-    def others(h):
-        spread_a.take(h)
-        spread_b.take(h)
-        for i, (level, there, _, _) in enumerate(at_distance(h)):
-            for s in spread_a.peers(level):
-                order.append((there, s))
-                multiply(f"o{h}_{i}", there, s)
-
-    column(0)
+            with jax.named_scope("fin"):
+                arrived(cond, rfar.at[s], sem_far.at[s])
+                when(cond, pack)
+                for i, chip in enumerate(far):
+                    send(
+                        cond, ysend.at[s, i], yrecv.at[s, i], sem_y.at[s, i],
+                        (me, chip * CORES + c),
+                    )
+
+    def multiply(pieces):
+        for piece in pieces:
+            multiply_far([piece])
+            multiply_near([piece])
+            finish([piece])
+
+    first = column(0)
+    second = column(1) if last else []
+    third = others(0)
+    multiply_far(first)
+    multiply_far(second)
+    finish(first)
     if last >= 2:
-        spread_b.forward(2)
+        spread_a.forward(2)
+        spread_b.forward(2, inner)
+    finish(second)
+    attend_later_blocks(near_blocks)
+    spread_b.forward_next()
+    attend_first_block(near_blocks)
+    if last >= 2:
+        spread_b.forward(2, at_end)
+    spread_a.take(0)
+    spread_b.take(0)
+    multiply_far(third)
+    pool(near_blocks)
+    finish(third)
+    spread_b.forward_side()
     spread_a.forward_side()
-    spread_b.forward_side()
-    if last:
-        column(1)
+    fourth = column(2) if last >= 2 else []
+    multiply_far(fourth)
+    multiply_near(first)
+    finish(fourth)
+
+    def only(cond, pieces):
+        return [(both(there, cond), s) for there, s in pieces]
+
+    order = first + second + third + fourth
+
+    def take_others(h, cond):
+        spread_a.take(h, cond)
+        spread_b.take(h, cond)
+        multiply(only(cond, others(h)))
+        order.extend(only(cond, others(h)))
+
+    if last > 1:
+        take_others(1, at_end)
     if last >= 3:
         spread_a.forward(3)
-    others(0)
+    multiply_near(second)
+    multiply_near(third)
+    multiply_near(fourth)
     if last >= 3:
         spread_b.forward(3)
+    for h in range(3, last + 1):
+        multiply(column(h))
+        order += column(h)
     for h in range(2, last):
-        column(h)
-        others(h)
+        take_others(h, None)
     if last > 1:
-        column(last)
+        take_others(1, inner)
     if last:
-        others(1)
-    if last > 1:
-        others(last)
+        take_others(last, None)
 
     with jax.named_scope("final"):
         w = wa.shape[2]
@@ -545,7 +685,7 @@
             when(cond, end)
 
     with jax.named_scope("wsend"):
-        for item in slots:
+        for item in slots + fixed:
             if item is not None:
                 when(item[0], item[1].wait_send)
 
@@ -572,8 +712,7 @@
     return pl.pallas_call(
         functools.partial(kernel, n_sp, n_tp, cols, len(ins), len(outs), widths),
         out_shape=pltpu.VMEM((rows, depth), BF16),
-        in_specs=[hbm, vmem, pl.BlockSpec(memory_space=pltpu.SMEM), vmem]
-        + [hbm] * (len(ins) + len(outs)),
+        in_specs=[hbm] * (4 + len(ins) + len(outs)),
         out_specs=vmem,
         scratch_shapes=[
             pltpu.VMEM((rows, depth), BF16),
@@ -587,6 +726,7 @@
             pltpu.VMEM((seq + WINDOW, width), BF16),
             pltpu.VMEM((seq, qw + pw), BF16),
             pltpu.VMEM((n_sp, 8, pw), F32),
+            pltpu.VMEM((seq // WINDOW, 8, pw), F32),
             pltpu.VMEM((8, pw), F32),
             pltpu.VMEM((n_sp, others, rows, out_cols), BF16),
             pltpu.VMEM((n_sp, others, rows, out_cols), BF16),
@@ -596,8 +736,12 @@
             pltpu.VMEM((n_sp, others, rows, out_cols), BF16),
             pltpu.VMEM((n_sp, others, rows, out_cols), F32),
             pltpu.VMEM((n_sp, rows, out_cols), F32),
-            dma((len(ins) + len(outs) + 1,)),
+            pltpu.VMEM((1, depth), F32),
+            pltpu.VMEM((1, pw), F32),
+            pltpu.SMEM(sink_logit.shape, F32),
+            dma((len(ins) + len(outs) + 4,)),
             dma((SEND_SLOTS,)),
+            dma((n_sp + 1,)),
             dma((n_sp,)),
             dma((n_sp,)),
             dma((n_sp,)),

time: 69.5 us -> 67.3 us (0.968)
  the two profiles are of different devices: /device:TPU:27 before, /device:TPU:0 now
where the time goes in v2:
time: 67.3 us; the launch traced here: 66 us
  Pallas kernels  65.1 us (97%)
  local copies, waits for them, and re-layouts  0.88 us (1%)
    pallas_call x1, Pallas kernels, local(): pl.pallas_call(functools.partial(kernel, n_sp, n_tp, cols, len(ins), len(...  65.1 us

profile of v2, /device:TPU:0, one launch (start us, length us, event | category | flops | bytes accessed | tf_op | source)
XLA Modules:
  0.0 66.0 jit_solution(9930686992950889678)
XLA Ops:
  0.0 65.1 %shard_map.100 = bf16[192,2048]{1,0:T(8,128)(2,1)S(1)} custom-call(bf16[192,2048]{1,0:T(8,128)(2,1)} %refs_0_.1, f32[1,2048]{1,0:T(1,128)} %bitcast.2, f32[4]{0:T(128)} %refs_2_.1, f32[1,256]{1,0:T(1,128)} %bitcast.3, bf16[256,256]{1,0:T(8,128)(2,1)} %refs_4_.1, bf16[256,128]{1,0:T(8,128)(2,1)} %refs_5_.1, bf16[256,128]{1,0:T(8,128)(2,1)} %refs_6_.1, ...), custom_call_target="tpu_custom_call" | custom-call | tf_op jit(solution)/shard_map/pallas_call | solution.py:712
  65.1 0.9 %copy.12 = bf16[192,2048]{1,0:T(8,128)(2,1)} copy(bf16[192,2048]{1,0:T(8,128)(2,1)S(1)} %shard_map.100) | data formatting | bytes 1572864

commit v3 on v2

--- a/solution.py
+++ b/solution.py
@@ -15,7 +15,8 @@
 EPS = 1e-06
 SHORT_REACHES = (8, 32)
 CORES = 2
-SEND_SLOTS = 40
+SEND_GROUPS = 19
+SIDE_SHARE = 0.375
 MESH = pl.DeviceIdType.MESH
 F32 = jnp.float32
 BF16 = jnp.bfloat16
@@ -39,7 +40,7 @@
     (
         out, tokv, xs, wq, wkv, wp, wa, wb, acc, ext, mix, tot, carry, given, dfar, rfar, dnear, rnear,
         ysend, yrecv, ofar, onear, gain, pgain, sink,
-        local_sem, send_sem, once_sem, sem_q, sem_kv, sem_p, sem_a, sem_b, sem_a_side,
+        local_sem, send_sem, sem_q, sem_kv, sem_p, sem_a, sem_b, sem_a_side,
         sem_tok, sem_halo, sem_tot, sem_far, sem_near, sem_y,
     ) = refs[4 + n_in + n_out :]
     qw, kw, vw, pw = widths
@@ -62,9 +63,6 @@
     ext[:WINDOW, qw:] = jnp.zeros((WINDOW, ext.shape[1] - qw), BF16)
 
     barrier = pltpu.get_barrier_semaphore()
-    next_row = jnp.logical_and(x == cols - 1, up)
-    last_row = jnp.logical_and(x == 0, down)
-
     def greet(cond, sp, tp):
         when(
             cond,
@@ -77,15 +75,10 @@
         greet(None, z * cols + (x + d) % cols, t)
     greet(up, me + cols, t)
     greet(down, me - cols, t)
-    greet_diagonal = cols > 1
-    if greet_diagonal:
-        greet(next_row, me + 1, t)
-        greet(last_row, me - 1, t)
-    for d in range(1, n_tp):
-        greet(None, me, (t + d) % n_tp)
-    expected = cols - 1 + n_tp - 1 + jnp.where(up, 1, 0) + jnp.where(down, 1, 0)
-    if greet_diagonal:
-        expected = expected + jnp.where(next_row, 1, 0) + jnp.where(last_row, 1, 0)
+    greet(None, me, partner)
+    for d in range(1, chips):
+        greet(None, me, (y + d) % chips * CORES + c)
+    expected = cols - 1 + chips + jnp.where(up, 1, 0) + jnp.where(down, 1, 0)
     locals_ = []
 
     def fetch(src, dst):
@@ -109,30 +102,38 @@
     with jax.named_scope("barrier"):
         pl.semaphore_wait(barrier, expected)
 
-    slots = [None] * send_sem.shape[0]
-    count = [0]
-
-    def send(cond, src, dst, recv, dev):
-        slot = count[0] % len(slots)
-        count[0] += 1
-        if slots[slot] is not None:
-            when(slots[slot][0], slots[slot][1].wait_send)
-        copy = pltpu.make_async_remote_copy(
-            src_ref=src, dst_ref=dst, send_sem=send_sem.at[slot], recv_sem=recv,
-            device_id=dev, device_id_type=MESH,
-        )
-        when(cond, copy.start)
-        slots[slot] = (cond, copy)
-
-    fixed = []
-
-    def send_once(cond, src, dst, sem, recv, dev):
-        copy = pltpu.make_async_remote_copy(
-            src_ref=src, dst_ref=dst, send_sem=sem, recv_sem=recv, device_id=dev,
-            device_id_type=MESH,
-        )
-        when(cond, copy.start)
-        fixed.append((cond, copy))
+    class Sends:
+        def __init__(self, whole):
+            self.whole, self.conds = whole, []
+            self.sem = send_sem.at[len(groups)]
+            groups.append(self)
+
+        def go(self, cond, src, dst, recv, dev):
+            copy = pltpu.make_async_remote_copy(
+                src_ref=src, dst_ref=dst, send_sem=self.sem, recv_sem=recv,
+                device_id=dev, device_id_type=MESH,
+            )
+            when(cond, copy.start)
+            self.conds.append((cond, copy))
+
+        def wait(self):
+            if self.whole is None:
+                for cond, copy in self.conds:
+                    when(cond, copy.wait_send)
+                return
+            sent = sum(1 if c is None else jnp.where(c, 1, 0) for c, _ in self.conds)
+            for n in range(1, min(len(self.conds), self.whole.shape[0]) + 1):
+                pl.when(sent == n)(functools.partial(self.wait_all, self.whole.at[pl.ds(0, n)]))
+
+        def wait_all(self, ref=None):
+            ref = self.whole if ref is None else ref
+            if self.conds:
+                pltpu.make_async_remote_copy(
+                    src_ref=ref, dst_ref=ref, send_sem=self.sem, recv_sem=send_sem.at[0],
+                    device_id=(me, partner), device_id_type=MESH,
+                ).wait_send()
+
+    groups = []
 
     def arrived(cond, dst, recv):
         copy = pltpu.make_async_remote_copy(
@@ -158,6 +159,11 @@
             self.side = int(k * share) // 16 * 16 if cols > 1 and levels > 1 else 0
             self.k, self.ends, self.next_too = k, ends, next_too and cols > 1 and last > 1
             self.have, self.have_at_ends = set(), set()
+            self.along_z, self.along_x = Sends(buf), Sends(buf)
+            self.part_z = self.part_x = None
+            if 0 < self.side < k:
+                self.part_z = Sends(buf.at[:, pl.ds(0, self.side), :])
+                self.part_x = Sends(buf.at[:, pl.ds(self.side, k - self.side), :])
 
         def piece(self, s, lo, hi):
             return self.buf.at[s] if (lo, hi) == (0, self.k) else self.buf.at[s, pl.ds(lo, hi - lo), :]
@@ -168,15 +174,20 @@
         def side_sems(self):
             return self.sem if self.side == self.k else self.side_sem
 
-        def go(self, cond, s, lo, hi, sem, dev_sp):
+        def go(self, cond, s, lo, hi, sem, dev_sp, over_x=False):
             ref = self.piece(s, lo, hi)
-            send(cond, ref, ref, sem.at[s], (dev_sp, t))
+            whole = (lo, hi) == (0, self.k)
+            if over_x:
+                sends = self.along_x if whole else self.part_x
+            else:
+                sends = self.along_z if whole else self.part_z
+            sends.go(cond, ref, ref, sem.at[s], (dev_sp, t))
 
         def across(self, cond, s, lo=0):
             if lo == self.k:
                 return
             for d in range(1, cols):
-                self.go(cond, s, lo, self.k, self.sem, z * cols + (x + d) % cols)
+                self.go(cond, s, lo, self.k, self.sem, z * cols + (x + d) % cols, True)
 
         def begin_up(self, cond=None):
             self.go(both(up, cond), me, 0, self.k, self.sem, me + cols)
@@ -201,7 +212,7 @@
         def peers(self, level):
             return [level * cols + (x + cols - d) % cols for d in range(1, cols)]
 
-        def forward_side(self):
+        def forward_side(self, cond=None):
             if not self.side:
                 return
             if not self.ends:
@@ -212,7 +223,7 @@
                     self.go(up, s, 0, self.side, sem, me + cols)
                     self.go(down, s, 0, self.side, sem, me - cols)
                     continue
-                self.go(at_end, s, 0, self.side, sem, (last - z) * cols + x)
+                self.go(cond, s, 0, self.side, sem, (last - z) * cols + x)
 
         def forward_next(self):
             if not self.next_too:
@@ -243,7 +254,7 @@
     spread_q = Spread("q", wq, sem_q, next_too=True)
     spread_kv = Spread("k", wkv, sem_kv, next_too=True)
     spread_p = Spread("p", wp, sem_p, 1.0)
-    spread_a = Spread("a", wa, sem_a, 0.5, sem_a_side, True, True)
+    spread_a = Spread("a", wa, sem_a, SIDE_SHARE, sem_a_side, True, True)
     spread_b = Spread("b", wb, sem_b, 1.0, None, True, True)
     for copy in locals_[:n_in]:
         copy.wait()
@@ -265,9 +276,12 @@
     def rows_of(device):
         return xs.at[:, pl.ds(pl.multiple_of(device * rows, rows), rows), :]
 
+    tokens_out = Sends(xs.at[:, pl.ds(0, (2 * chips - 1) * rows), :])
     for d in range(1, chips):
-        send(None, rows_of(t), rows_of(t), sem_tok.at[t], (me, (y + d) % chips * CORES + c))
-    send(None, rows_of(t), rows_of(t), sem_tok.at[t], (me, partner))
+        tokens_out.go(
+            None, rows_of(t), rows_of(t), sem_tok.at[t], (me, (y + d) % chips * CORES + c)
+        )
+    tokens_out.go(None, rows_of(t), rows_of(t), sem_tok.at[t], (me, partner))
 
     def chip_rows(chip):
         return pl.ds(pl.multiple_of(chip * per, per), per)
@@ -316,7 +330,7 @@
             for d in range(1, chips):
                 at = (y + chips - d) % chips * CORES + c
                 arrived(None, rows_of(at), sem_tok.at[at])
-                send(None, rows_of(at), rows_of(at), sem_tok.at[at], (me, partner))
+                tokens_out.go(None, rows_of(at), rows_of(at), sem_tok.at[at], (me, partner))
 
     def take_tokens():
         with jax.named_scope("tokt"):
@@ -374,12 +388,12 @@
     with jax.named_scope("settleq"):
         settle(0, channel0)
 
+    halo_out, tot_out = [Sends(None), Sends(None)], Sends(tot)
+
     def pass_on(cond, at, width, n, i):
         head = ext.at[pl.ds(WINDOW - n, n), pl.ds(at, width)]
         tail = ext.at[pl.ds(seq + WINDOW - n, n), pl.ds(at, width)]
-        send_once(
-            both(cond, later), tail, head, once_sem.at[i], sem_halo.at[i], (me + 1, t)
-        )
+        halo_out[i].go(both(cond, later), tail, head, sem_halo.at[i], (me + 1, t))
         return head
 
     head_kv = pass_on(None, qw, kw + vw, WINDOW, 0)
@@ -412,9 +426,9 @@
         for is_group, n in halos:
             pass_on(both(is_group, cond), channel0, pw, n, 1)
         for d in range(1, n_sp):
-            send_once(
+            tot_out.go(
                 both(both(whole_prefix, cond), me + d < n_sp), tot.at[me], tot.at[me],
-                once_sem.at[1 + d], sem_tot.at[me], (me + d, t),
+                sem_tot.at[0], (me + d, t),
             )
 
     finish_pool_rows(inner)
@@ -536,13 +550,13 @@
             head = ext.at[pl.ds(WINDOW - n, n), pl.ds(channel0, pw)]
             arrived(both(cond, earlier), head, sem_halo.at[1])
         given[...] = jnp.zeros(given.shape, F32)
-        for d in range(1, n_sp):
-
-            def add(d=d):
-                arrived(None, tot.at[me - d], sem_tot.at[me - d])
-                given[...] += tot[me - d]
-
-            when(both(whole_prefix, me - d >= 0), add)
+        for n in range(1, n_sp):
+
+            def add(n=n):
+                arrived(None, tot.at[pl.ds(0, n)], sem_tot.at[0])
+                given[...] = jnp.sum(tot[:n], axis=0)
+
+            when(both(whole_prefix, me == n), add)
     pool(far_blocks)
 
     def product(s, chip, core):
@@ -561,6 +575,8 @@
             for s in spread_a.peers(level)
         ]
 
+    far_out, near_out, y_out = Sends(dfar), Sends(dnear), Sends(ysend)
+
     def multiply_far(pieces):
         for cond, s in pieces if chips > 1 else ():
 
@@ -574,7 +590,7 @@
 
             with jax.named_scope("mulf"):
                 when(cond, give)
-                send(cond, dfar.at[s], rfar.at[s], sem_far.at[s], (me, partner))
+                far_out.go(cond, dfar.at[s], rfar.at[s], sem_far.at[s], (me, partner))
                 when(cond, keep)
 
     def multiply_near(pieces):
@@ -588,7 +604,7 @@
 
             with jax.named_scope("muln"):
                 when(cond, give_near)
-                send(cond, dnear.at[s], rnear.at[s], sem_near.at[s], (me, partner))
+                near_out.go(cond, dnear.at[s], rnear.at[s], sem_near.at[0], (me, partner))
                 when(cond, keep_near)
 
     def finish(pieces):
@@ -602,7 +618,7 @@
                 arrived(cond, rfar.at[s], sem_far.at[s])
                 when(cond, pack)
                 for i, chip in enumerate(far):
-                    send(
+                    y_out.go(
                         cond, ysend.at[s, i], yrecv.at[s, i], sem_y.at[s, i],
                         (me, chip * CORES + c),
                     )
@@ -630,11 +646,11 @@
         spread_b.forward(2, at_end)
     spread_a.take(0)
     spread_b.take(0)
+    spread_b.forward_side(z == last)
+    spread_a.forward_side(z == last)
     multiply_far(third)
     pool(near_blocks)
     finish(third)
-    spread_b.forward_side()
-    spread_a.forward_side()
     fourth = column(2) if last >= 2 else []
     multiply_far(fourth)
     multiply_near(first)
@@ -655,27 +671,44 @@
         take_others(1, at_end)
     if last >= 3:
         spread_a.forward(3)
+    spread_b.forward_side(z == 0)
+    spread_a.forward_side(z == 0)
     multiply_near(second)
-    multiply_near(third)
-    multiply_near(fourth)
     if last >= 3:
         spread_b.forward(3)
+    left = third + fourth
     for h in range(3, last + 1):
-        multiply(column(h))
+        multiply_far(column(h))
+        multiply_near(left[:1])
+        finish(column(h))
+        left = left[1:] + column(h)
         order += column(h)
     for h in range(2, last):
-        take_others(h, None)
+        spread_a.take(h)
+        spread_b.take(h)
+        multiply_far(others(h))
+        multiply_near(left[:2])
+        finish(others(h))
+        left = left[2:] + others(h)
+        order += others(h)
+    multiply_near(left)
     if last > 1:
         take_others(1, inner)
     if last:
         take_others(last, None)
 
+    with jax.named_scope("wsend"):
+        for sends in groups:
+            if sends is tokens_out:
+                sends.wait_all()
+            elif sends not in (far_out, near_out, y_out):
+                sends.wait()
     with jax.named_scope("final"):
+        arrived(None, rnear, sem_near.at[0])
         w = wa.shape[2]
         for cond, s in order:
 
             def end(s=s):
-                arrived(None, rnear.at[s], sem_near.at[s])
                 value = onear[s] + rnear[s].astype(F32)
                 for i in range(chips - 1):
                     arrived(None, yrecv.at[s, i], sem_y.at[s, i])
@@ -684,10 +717,8 @@
 
             when(cond, end)
 
-    with jax.named_scope("wsend"):
-        for item in slots + fixed:
-            if item is not None:
-                when(item[0], item[1].wait_send)
+    for sends in (far_out, near_out, y_out):
+        sends.wait_all()
 
 
 def local(
@@ -740,8 +771,7 @@
             pltpu.VMEM((1, pw), F32),
             pltpu.SMEM(sink_logit.shape, F32),
             dma((len(ins) + len(outs) + 4,)),
-            dma((SEND_SLOTS,)),
-            dma((n_sp + 1,)),
+            dma((SEND_GROUPS,)),
             dma((n_sp,)),
             dma((n_sp,)),
             dma((n_sp,)),
@@ -750,9 +780,9 @@
             dma((n_sp,)),
             dma((n_tp,)),
             dma((2,)),
+            dma((1,)),
             dma((n_sp,)),
-            dma((n_sp,)),
-            dma((n_sp,)),
+            dma((1,)),
             dma((n_sp, others)),
         ],
         compiler_params=pltpu.CompilerParams(

time: 67.3 us -> 65.1 us (0.967); the launches traced: 66 us -> 64.8 us
  Pallas kernels: 65.1 us -> 63.9 us
    pallas_call x1, Pallas kernels: 65.1 us -> 63.9 us  [local(): pl.pallas_call(functools.partial(kernel, n_sp, n_tp, cols, len(ins), len(...]
where the time goes in v3:
time: 65.1 us; the launch traced here: 64.8 us
  Pallas kernels  63.9 us (98%)
  local copies, waits for them, and re-layouts  0.88 us (1%)
    pallas_call x1, Pallas kernels, local(): pl.pallas_call(functools.partial(kernel, n_sp, n_tp, cols, len(ins), len(...  63.9 us

profile of v3, /device:TPU:0, one launch (start us, length us, event | category | flops | bytes accessed | tf_op | source)
XLA Modules:
  0.0 64.8 jit_solution(14519202368016103756)
XLA Ops:
  0.0 63.9 %shard_map.100 = bf16[192,2048]{1,0:T(8,128)(2,1)S(1)} custom-call(bf16[192,2048]{1,0:T(8,128)(2,1)} %refs_0_.1, f32[1,2048]{1,0:T(1,128)} %bitcast.2, f32[4]{0:T(128)} %refs_2_.1, f32[1,256]{1,0:T(1,128)} %bitcast.3, bf16[256,256]{1,0:T(8,128)(2,1)} %refs_4_.1, bf16[256,128]{1,0:T(8,128)(2,1)} %refs_5_.1, bf16[256,128]{1,0:T(8,128)(2,1)} %refs_6_.1, ...), custom_call_target="tpu_custom_call" | custom-call | tf_op jit(solution)/shard_map/pallas_call | solution.py:743
  63.9 0.9 %copy.12 = bf16[192,2048]{1,0:T(8,128)(2,1)} copy(bf16[192,2048]{1,0:T(8,128)(2,1)S(1)} %shard_map.100) | data formatting | bytes 1572864

commit v4 on v2

v4 whole, which is shorter than its diff:
```python
import functools
import math

import jax
import jax.numpy as jnp
from jax import lax
from jax.experimental import pallas as pl
from jax.experimental.pallas import tpu as pltpu
from jax.sharding import PartitionSpec as P

HEAD_DIM = 64
POOL_CH = 256
POOL_GROUPS = 4
WINDOW = 128
EPS = 1e-06
SHORT_REACHES = (8, 32)
CORES = 2
SEND_GROUPS = 17
SIDE_SHARE = 0.375
MESH = pl.DeviceIdType.MESH
F32 = jnp.float32
BF16 = jnp.bfloat16


def when(cond, fn):
    if cond is None:
        fn()
    else:
        pl.when(cond)(fn)


def both(a, b):
    return b if a is None else (a if b is None else jnp.logical_and(a, b))


def layer(n_sp, n_tp, cols, n_in, n_out, widths, refs, late_sem, sem_near, sem_y):
    tok, gain_in, sink_in, pgain_in = refs[:4]
    win_refs = refs[4 : 4 + n_in]
    wout_refs = refs[4 + n_in : 4 + n_in + n_out]
    (
        out, tokv, xs, wq, wkv, wp, wa, wb, acc, ext, mix, tot, carry, given, dfar, rfar, dnear, rnear,
        ysend, yrecv, ofar, onear, gain, pgain, sink,
    ) = refs[4 + n_in + n_out :]
    qw, kw, vw, pw = widths
    levels = n_sp // cols
    chips = n_tp // CORES
    rows, seq = tok.shape[0], xs.shape[1]
    per = rows * CORES
    channel0 = qw + kw + vw
    blocks = seq // WINDOW
    me, t = lax.axis_index("sp"), lax.axis_index("tp")
    z, x = me // cols, me % cols
    y, c = t // CORES, t % CORES
    partner = y * CORES + (1 - c)
    up, down = z + 1 < levels, z > 0
    later, earlier = me + 1 < n_sp, me > 0
    last = levels - 1
    at_end = jnp.logical_or(z == 0, z == last)
    inner = jnp.logical_not(at_end)

    def arrived(cond, dst, recv):
        copy = pltpu.make_async_remote_copy(
            src_ref=dst, dst_ref=dst, send_sem=late_sem.at[0], recv_sem=recv,
            device_id=(me, partner), device_id_type=MESH,
        )
        when(cond, copy.wait_recv)

    def at_distance(h):
        if h == 0:
            return ((z, None, None, None),)
        return (
            (z - h, z - h >= 0, up, me + cols),
            (z + h, z + h < levels, down, me - cols),
        )

    def peers(level):
        return [level * cols + (x + cols - d) % cols for d in range(1, cols)]

    def column(h):
        return [(there, level * cols + x) for level, there, _, _ in at_distance(h)]

    def others(h):
        return [
            (there, s)
            for level, there, _, _ in at_distance(h)
            for s in peers(level)
        ]

    near = [y]
    far = [(y + d) % chips for d in range(1, chips)]

    def gather_and_multiply(
        local_sem, send_sem, sem_q, sem_kv, sem_p, sem_a, sem_b, sem_a_side, sem_tok, sem_halo,
        sem_tot, sem_far,
    ):
        ext[:WINDOW, qw:] = jnp.zeros((WINDOW, ext.shape[1] - qw), BF16)

        barrier = pltpu.get_barrier_semaphore()

        def greet(cond, sp, tp):
            when(
                cond,
                lambda: pl.semaphore_signal(
                    barrier, inc=1, device_id=(sp, tp), device_id_type=MESH
                ),
            )

        for d in range(1, cols):
            greet(None, z * cols + (x + d) % cols, t)
        greet(up, me + cols, t)
        greet(down, me - cols, t)
        greet(None, me, partner)
        for d in range(1, chips):
            greet(None, me, (y + d) % chips * CORES + c)
        expected = cols - 1 + chips + jnp.where(up, 1, 0) + jnp.where(down, 1, 0)

        locals_ = []

        def fetch(src, dst):
            copy = pltpu.make_async_copy(src, dst, local_sem.at[len(locals_)])
            copy.start()
            locals_.append(copy)

        fetch(win_refs[0], wq.at[me])
        at = 0
        for ref in win_refs[1:-1]:
            w = ref.shape[1]
            fetch(ref, wkv.at[me, :, pl.ds(at, w)])
            at += w
        fetch(win_refs[-1], wp.at[me])
        fetch(tok, tokv)
        fetch(gain_in, gain)
        fetch(wout_refs[0], wa.at[me])
        fetch(wout_refs[1], wb.at[me])
        fetch(pgain_in, pgain)
        fetch(sink_in, sink)
        pl.semaphore_wait(barrier, expected)

        class Sends:
            def __init__(self, whole, sem=None):
                self.whole, self.conds, self.sem = whole, [], sem
                if sem is None:
                    self.sem = send_sem.at[len(groups)]
                    groups.append(self)

            def go(self, cond, src, dst, recv, dev):
                copy = pltpu.make_async_remote_copy(
                    src_ref=src, dst_ref=dst, send_sem=self.sem, recv_sem=recv,
                    device_id=dev, device_id_type=MESH,
                )
                when(cond, copy.start)
                self.conds.append((cond, copy))

            def wait(self):
                if self.whole is None:
                    for cond, copy in self.conds:
                        when(cond, copy.wait_send)
                    return
                sent = sum(1 if c is None else jnp.where(c, 1, 0) for c, _ in self.conds)
                for n in range(1, min(len(self.conds), self.whole.shape[0]) + 1):
                    pl.when(sent == n)(functools.partial(self.wait_all, self.whole.at[pl.ds(0, n)]))

            def wait_all(self, ref=None):
                ref = self.whole if ref is None else ref
                if self.conds:
                    pltpu.make_async_remote_copy(
                        src_ref=ref, dst_ref=ref, send_sem=self.sem, recv_sem=send_sem.at[0],
                        device_id=(me, partner), device_id_type=MESH,
                    ).wait_send()

        groups = []

        class Spread:
            def __init__(
                self, name, buf, sem, share=0.0, side_sem=None, ends=False, next_too=False
            ):
                self.name, self.buf, self.sem, self.side_sem = name, buf, sem, side_sem
                k = buf.shape[1]
                self.side = int(k * share) // 16 * 16 if cols > 1 and levels > 1 else 0
                self.k, self.ends, self.next_too = k, ends, next_too and cols > 1 and last > 1
                self.have, self.have_at_ends = set(), set()
                self.along_z, self.along_x = Sends(buf), Sends(buf)
                self.part_z = self.part_x = None
                if 0 < self.side < k:
                    self.part_z = Sends(buf.at[:, pl.ds(0, self.side), :])
                    self.part_x = Sends(buf.at[:, pl.ds(self.side, k - self.side), :])

            def piece(self, s, lo, hi):
                return self.buf.at[s] if (lo, hi) == (0, self.k) else self.buf.at[s, pl.ds(lo, hi - lo), :]

            def side_at(self, h):
                return self.side if h == (last if self.ends else 1) else 0

            def side_sems(self):
                return self.sem if self.side == self.k else self.side_sem

            def go(self, cond, s, lo, hi, sem, dev_sp, over_x=False):
                ref = self.piece(s, lo, hi)
                whole = (lo, hi) == (0, self.k)
                if over_x:
                    sends = self.along_x if whole else self.part_x
                else:
                    sends = self.along_z if whole else self.part_z
                sends.go(cond, ref, ref, sem.at[s], (dev_sp, t))

            def across(self, cond, s, lo=0):
                if lo == self.k:
                    return
                for d in range(1, cols):
                    self.go(cond, s, lo, self.k, self.sem, z * cols + (x + d) % cols, True)

            def begin_up(self, cond=None):
                self.go(both(up, cond), me, 0, self.k, self.sem, me + cols)

            def begin_down(self):
                self.go(down, me, 0, self.k, self.sem, me - cols)

            def begin_x(self, cond=None):
                self.across(cond, me)

            def forward(self, h, cond=None):
                for level, there, on, to in at_distance(h):
                    there = both(there, cond)
                    s = level * cols + x
                    arrived(there, self.buf.at[s], self.sem.at[s])
                    self.go(both(there, on), s, 0, self.k, self.sem, to)
                    if self.next_too and h == 1:
                        there = both(there, jnp.logical_and(level != 0, level != last))
                    self.across(there, s, self.side_at(h))

            def forward_side(self, cond=None):
                if not self.side:
                    return
                if not self.ends:
                    self.take(0)
                sem = self.side_sems()
                for s in peers(z):
                    if not self.ends:
                        self.go(up, s, 0, self.side, sem, me + cols)
                        self.go(down, s, 0, self.side, sem, me - cols)
                        continue
                    self.go(cond, s, 0, self.side, sem, (last - z) * cols + x)

            def forward_next(self):
                if not self.next_too:
                    return
                self.take(0, at_end)
                for s in peers(z):
                    self.go(z == 0, s, 0, self.k, self.sem, me + cols)
                    self.go(z == last, s, 0, self.k, self.sem, me - cols)

            def take(self, h, cond=None):
                if h in self.have or (h in self.have_at_ends and cond is at_end):
                    return
                if cond is at_end:
                    self.have_at_ends.add(h)
                else:
                    self.have.add(h)
                    cond = inner if h in self.have_at_ends else cond
                side = self.side_at(h)
                for level, there, _, _ in at_distance(h):
                    there = both(there, cond)
                    for s in peers(level):
                        if side:
                            arrived(there, self.piece(s, 0, side), self.side_sems().at[s])
                        if side < self.k:
                            arrived(there, self.piece(s, side, self.k), self.sem.at[s])

        spread_q = Spread("q", wq, sem_q, next_too=True)
        spread_kv = Spread("k", wkv, sem_kv, next_too=True)
        spread_p = Spread("p", wp, sem_p, 1.0)
        spread_a = Spread("a", wa, sem_a, SIDE_SHARE, sem_a_side, True, True)
        spread_b = Spread("b", wb, sem_b, 1.0, None, True, True)
        for copy in locals_[:n_in]:
            copy.wait()
        for spread in (spread_q, spread_kv, spread_p):
            spread.begin_up()
            spread.begin_down()
            spread.begin_x()
        locals_[n_in].wait()
        locals_[n_in + 1].wait()

        mine = pl.ds(pl.multiple_of(t * rows, rows), rows)
        wide = tokv[...].astype(F32)
        inverse = lax.rsqrt(jnp.mean(wide * wide, axis=1, keepdims=True) + EPS)
        piece = xs.shape[2]
        for i in range(n_sp):
            span = slice(i * piece, (i + 1) * piece)
            xs[i, mine, :] = (tokv[:, span].astype(F32) * inverse * gain[:, span]).astype(BF16)

        def rows_of(device):
            return xs.at[:, pl.ds(pl.multiple_of(device * rows, rows), rows), :]

        tokens_out = Sends(xs.at[:, pl.ds(0, (2 * chips - 1) * rows), :])
        for d in range(1, chips):
            tokens_out.go(
                None, rows_of(t), rows_of(t), sem_tok.at[t], (me, (y + d) % chips * CORES + c)
            )
        tokens_out.go(None, rows_of(t), rows_of(t), sem_tok.at[t], (me, partner))

        def chip_rows(chip):
            return pl.ds(pl.multiple_of(chip * per, per), per)

        def project(spread, at, h, which):
            spread.take(h)
            w = spread.buf.shape[2]
            for level, there, _, _ in at_distance(h):

                def run(level=level):
                    for chip in which:
                        r = chip_rows(chip)
                        value = None
                        for i in range(cols):
                            s = level * cols + i
                            part = jnp.dot(
                                xs[s, r, :], spread.buf[s], preferred_element_type=F32
                            )
                            value = part if value is None else value + part
                        if h == 0:
                            acc[r, at : at + w] = value
                        else:
                            acc[r, at : at + w] += value

                when(there, run)

        def project_q(h, which):
            project(spread_q, 0, h, which)

        def project_kv(h, which):
            project(spread_kv, qw, h, which)

        def project_p(h, which):
            project(spread_p, channel0, h, which)

        arrived(None, rows_of(partner), sem_tok.at[partner])
        for copy in locals_[n_in + 2 :]:
            copy.wait()

        def gather_tokens():
            for d in range(1, chips):
                at = (y + chips - d) % chips * CORES + c
                arrived(None, rows_of(at), sem_tok.at[at])
                tokens_out.go(None, rows_of(at), rows_of(at), sem_tok.at[at], (me, partner))

        def take_tokens():
            for d in range(1, chips):
                at = (y + chips - d) % chips * CORES + (1 - c)
                arrived(None, rows_of(at), sem_tok.at[at])

        for h in range(1, last):
            spread_q.forward(h)
            if h > 1:
                project_p(h - 2, near)
            spread_kv.forward(h)
            if h == 1:
                spread_q.forward_next()
            project_q(h - 1, near)
            spread_p.forward(h)
            if h == 1:
                spread_kv.forward_next()
            project_kv(h - 1, near)
        spread_p.forward_side()
        spread_a.begin_down()
        spread_a.begin_up()
        spread_b.begin_down()
        spread_b.begin_up(at_end)
        gather_tokens()
        done = max(0, last - 1)
        if last:
            spread_q.forward(last)
        take_tokens()
        for h in range(done):
            project_q(h, far)
            project_kv(h, far)
        for h in range(max(0, last - 2)):
            project_p(h, far)
        if last:
            spread_kv.forward(last)
        for h in range(done, last):
            project_q(h, near + far)
            project_kv(h, near + far)
        if last:
            spread_p.forward(last)
        for h in range(max(0, last - 2), last):
            if h != 1:
                project_p(h, near + far)
        project_q(last, far + near)
        if last:
            project_p(1, far + near)
        project_kv(last, far + near)

        def settle(lo, hi):
            for chip in range(chips):
                r = slice(chip * per, (chip + 1) * per)
                ext[WINDOW + chip * per : WINDOW + (chip + 1) * per, lo:hi] = acc[r, lo:hi].astype(BF16)

        settle(0, channel0)

        halo_out, tot_out = [Sends(None), Sends(None)], Sends(tot)

        def pass_on(cond, at, width, n, i):
            head = ext.at[pl.ds(WINDOW - n, n), pl.ds(at, width)]
            tail = ext.at[pl.ds(seq + WINDOW - n, n), pl.ds(at, width)]
            halo_out[i].go(both(cond, later), tail, head, sem_halo.at[i], (me + 1, t))
            return head

        head_kv = pass_on(None, qw, kw + vw, WINDOW, 0)

        group = t * pw // POOL_CH
        whole_prefix = group == POOL_GROUPS - 1
        halos = [
            (group == g, -(-(reach - 1) // 16) * 16)
            for g, reach in enumerate(SHORT_REACHES + (WINDOW,))
        ]

        def finish_pool_rows(cond):
            def run():
                settle(channel0, ext.shape[1])
                for n in range(blocks):
                    r = slice(WINDOW + n * WINDOW, 2 * WINDOW + n * WINDOW)
                    total = jnp.sum(ext[r, channel0:].astype(F32), axis=0, keepdims=True)
                    if n + 1 < blocks:
                        carry[n + 1] = jnp.broadcast_to(
                            total if n == 0 else carry[n, 0:1, :] + total, carry.shape[1:]
                        )
                    else:
                        tot[me] = jnp.broadcast_to(
                            total if n == 0 else carry[n, 0:1, :] + total, tot.shape[1:]
                        )
                carry[0] = jnp.zeros(carry.shape[1:], F32)

            when(cond, run)
            for is_group, n in halos:
                pass_on(both(is_group, cond), channel0, pw, n, 1)
            for d in range(1, n_sp):
                tot_out.go(
                    both(both(whole_prefix, cond), me + d < n_sp), tot.at[me], tot.at[me],
                    sem_tot.at[0], (me + d, t),
                )

        finish_pool_rows(inner)
        spread_a.begin_x()
        spread_b.begin_x(inner)
        spread_b.begin_up(inner)
        if last:
            spread_a.forward(1, inner)

        group_heads = qw // kw
        stacked = group_heads * WINDOW
        scale = HEAD_DIM ** (-0.5)

        def attend(n):
            q_rows = pl.ds(pl.multiple_of(n * WINDOW + WINDOW, WINDOW), WINDOW)
            k_rows = pl.ds(pl.multiple_of(n * WINDOW, WINDOW), 2 * WINDOW)
            queries = ext[q_rows, :qw]
            keys = ext[k_rows, qw : qw + kw]
            values = ext[k_rows, qw + kw : channel0]
            row = lax.broadcasted_iota(jnp.int32, (stacked, 2 * WINDOW), 0)
            q_index = row % WINDOW
            k_index = lax.broadcasted_iota(jnp.int32, (stacked, 2 * WINDOW), 1)
            lowest = jnp.where(me * blocks + n == 0, WINDOW, 0)
            allowed = (k_index > q_index) & (k_index <= q_index + WINDOW) & (k_index >= lowest)
            which = lax.broadcasted_iota(jnp.int32, (stacked, 1), 0) // WINDOW
            done = []
            for j in range(kw // HEAD_DIM):
                part = slice(j * HEAD_DIM, (j + 1) * HEAD_DIM)
                first = j * group_heads
                q = jnp.concatenate(
                    [
                        queries[:, (first + g) * HEAD_DIM : (first + g + 1) * HEAD_DIM]
                        for g in range(group_heads)
                    ],
                    axis=0,
                )
                scores = (
                    lax.dot_general(
                        q, keys[:, part], (((1,), (1,)), ((), ())), preferred_element_type=F32
                    )
                    * scale
                )
                scores = jnp.where(allowed, scores, -jnp.inf)
                sinks = jnp.full((stacked, 1), sink[first], F32)
                for g in range(1, group_heads):
                    sinks = jnp.where(which == g, sink[first + g], sinks)
                peak = jnp.maximum(jnp.max(scores, axis=1, keepdims=True), sinks)
                expo = jnp.exp(scores - peak)
                denom = jnp.sum(expo, axis=1, keepdims=True) + jnp.exp(sinks - peak)
                probs = (expo * (1.0 / denom)).astype(BF16)
                got = jnp.dot(probs, values[:, part], preferred_element_type=F32)
                done += [got[g * WINDOW : (g + 1) * WINDOW] for g in range(group_heads)]
            to = pl.ds(pl.multiple_of(n * WINDOW, WINDOW), WINDOW)
            mix[to, :qw] = jnp.concatenate(done, axis=1).astype(BF16)

        if per % WINDOW == 0:
            span = per // WINDOW
            far_blocks, near_blocks = [chip * span for chip in far], [y * span]
        else:
            span = blocks
            far_blocks, near_blocks = [0], []

        def attend_later_blocks(firsts):
            for first in firsts:
                pl.loop(1, span)(lambda i, first=first: attend(first + i))

        def attend_first_block(firsts):
            for first in firsts:
                cond = earlier if isinstance(first, int) else both(earlier, first == 0)
                arrived(cond, head_kv, sem_halo.at[0])
                attend(first)

        reach = jnp.where(
            group == 0, SHORT_REACHES[0], jnp.where(group == 1, SHORT_REACHES[1], WINDOW)
        )
        reach = jnp.where(whole_prefix, n_sp * seq, reach)
        lowest = jnp.where(whole_prefix, WINDOW, 0)

        def pool(firsts):
            for first in firsts:

                @pl.loop(0, span)
                def _(i, first=first):
                    n = first + i
                    q_index = lax.broadcasted_iota(jnp.int32, (WINDOW, 2 * WINDOW), 0)
                    k_index = lax.broadcasted_iota(jnp.int32, (WINDOW, 2 * WINDOW), 1)
                    distance = q_index + WINDOW - k_index
                    band = (distance >= 0) & (distance < reach) & (k_index >= lowest)
                    band = jnp.where(band, 1.0, 0.0).astype(BF16)
                    k_rows = pl.ds(pl.multiple_of(n * WINDOW, WINDOW), 2 * WINDOW)
                    both_blocks = ext[k_rows, channel0:]
                    before = jnp.where(whole_prefix, carry[n, 0:1, :] + given[0:1, :], 0.0)
                    sums = jnp.dot(band, both_blocks, preferred_element_type=F32) + before
                    position = (
                        me * seq + n * WINDOW + lax.broadcasted_iota(jnp.int32, (WINDOW, 1), 0)
                    )
                    counted = jnp.minimum(position + 1, reach).astype(F32)
                    mixed = (sums / counted - both_blocks[WINDOW:].astype(F32)) * pgain[...]
                    to = pl.ds(pl.multiple_of(n * WINDOW, WINDOW), WINDOW)
                    mix[to, qw:] = mixed.astype(BF16)

        attend_later_blocks(far_blocks)
        if last >= 2:
            project_p(last, far + near)
        finish_pool_rows(at_end)
        spread_b.begin_x(at_end)
        if last:
            spread_a.forward(1, at_end)
            spread_b.forward(1, inner)
        attend_first_block(far_blocks)
        if last:
            spread_b.forward(1, at_end)
        spread_a.forward_next()
        for cond, n in halos:
            head = ext.at[pl.ds(WINDOW - n, n), pl.ds(channel0, pw)]
            arrived(both(cond, earlier), head, sem_halo.at[1])
        given[...] = jnp.zeros(given.shape, F32)
        for n in range(1, n_sp):

            def add(n=n):
                arrived(None, tot.at[pl.ds(0, n)], sem_tot.at[0])
                given[...] = jnp.sum(tot[:n], axis=0)

            when(both(whole_prefix, me == n), add)
        pool(far_blocks)

        def product(s, chip, core):
            r = pl.ds(pl.multiple_of((chip * CORES + core) * rows, rows), rows)
            return jnp.dot(mix[r, :qw], wa[s], preferred_element_type=F32) + jnp.dot(
                mix[r, qw:], wb[s], preferred_element_type=F32
            )

        far_out = Sends(dfar)
        near_out, y_out = Sends(dnear, late_sem.at[0]), Sends(ysend, late_sem.at[1])

        def multiply_far(pieces):
            for cond, s in pieces if chips > 1 else ():

                def give(s=s):
                    for i, chip in enumerate(far):
                        dfar[s, i] = product(s, chip, 1 - c).astype(BF16)

                def keep(s=s):
                    for i, chip in enumerate(far):
                        ofar[s, i] = product(s, chip, c)

                when(cond, give)
                far_out.go(cond, dfar.at[s], rfar.at[s], sem_far.at[s], (me, partner))
                when(cond, keep)

        def multiply_near(pieces):
            for cond, s in pieces:

                def give_near(s=s):
                    dnear[s] = product(s, y, 1 - c).astype(BF16)

                def keep_near(s=s):
                    onear[s] = product(s, y, c)

                when(cond, give_near)
                near_out.go(cond, dnear.at[s], rnear.at[s], sem_near.at[0], (me, partner))
                when(cond, keep_near)

        def finish(pieces):
            for cond, s in pieces if chips > 1 else ():

                def pack(s=s):
                    for i in range(chips - 1):
                        ysend[s, i] = (ofar[s, i] + rfar[s, i].astype(F32)).astype(BF16)

                arrived(cond, rfar.at[s], sem_far.at[s])
                when(cond, pack)
                for i, chip in enumerate(far):
                    y_out.go(
                        cond, ysend.at[s, i], yrecv.at[s, i], sem_y.at[s, i],
                        (me, chip * CORES + c),
                    )

        def multiply(pieces):
            for piece in pieces:
                multiply_far([piece])
                multiply_near([piece])
                finish([piece])

        first = column(0)
        second = column(1) if last else []
        third = others(0)
        multiply_far(first)
        multiply_far(second)
        finish(first)
        if last >= 2:
            spread_a.forward(2)
            spread_b.forward(2, inner)
        finish(second)
        attend_later_blocks(near_blocks)
        spread_b.forward_next()
        attend_first_block(near_blocks)
        if last >= 2:
            spread_b.forward(2, at_end)
        spread_a.take(0)
        spread_b.take(0)
        spread_b.forward_side(z == last)
        spread_a.forward_side(z == last)
        multiply_far(third)
        pool(near_blocks)
        finish(third)
        fourth = column(2) if last >= 2 else []
        multiply_far(fourth)
        multiply_near(first)
        finish(fourth)

        def only(cond, pieces):
            return [(both(there, cond), s) for there, s in pieces]


        def take_others(h, cond):
            spread_a.take(h, cond)
            spread_b.take(h, cond)
            multiply(only(cond, others(h)))

        if last > 1:
            take_others(1, at_end)
        if last >= 3:
            spread_a.forward(3)
        spread_b.forward_side(z == 0)
        spread_a.forward_side(z == 0)
        multiply_near(second)
        if last >= 3:
            spread_b.forward(3)
        left = third + fourth
        for h in range(3, last + 1):
            multiply_far(column(h))
            multiply_near(left[:1])
            finish(column(h))
            left = left[1:] + column(h)
        for h in range(2, last):
            spread_a.take(h)
            spread_b.take(h)
            multiply_far(others(h))
            multiply_near(left[:2])
            finish(others(h))
            left = left[2:] + others(h)
        multiply_near(left)
        if last > 1:
            take_others(1, inner)
        if last:
            take_others(last, None)

        for sends in groups:
            if sends is tokens_out:
                sends.wait_all()
            elif sends is far_out:
                sends.wait_all()
            else:
                sends.wait()
    dma = pltpu.SemaphoreType.DMA
    per_shard = dma((n_sp,))
    pl.run_scoped(
        gather_and_multiply, dma((n_in + n_out + 4,)), dma((SEND_GROUPS,)), per_shard, per_shard,
        per_shard, per_shard, per_shard, per_shard, dma((n_tp,)), dma((2,)), dma((1,)), per_shard,
    )

    order = column(0)
    if last:
        order = order + column(1)
    order = order + others(0)
    for h in range(2, last + 1):
        order = order + column(h)
    for h in range(1, last + 1):
        order = order + others(h)

    arrived(None, rnear, sem_near.at[0])
    w = wa.shape[2]
    for cond, s in order:

        def end(s=s):
            value = onear[s] + rnear[s].astype(F32)
            for i in range(chips - 1):
                arrived(None, yrecv.at[s, i], sem_y.at[s, i])
                value += yrecv[s, i].astype(F32)
            out[:, pl.ds(pl.multiple_of(s * w, w), w)] = value.astype(BF16)

        when(cond, end)

    for ref, i in ((dnear, 0), (ysend, 1)) if chips > 1 else ((dnear, 0),):
        pltpu.make_async_remote_copy(
            src_ref=ref, dst_ref=ref, send_sem=late_sem.at[i], recv_sem=sem_near.at[0],
            device_id=(me, partner), device_id_type=MESH,
        ).wait_send()


def kernel(n_sp, n_tp, cols, n_in, n_out, widths, *refs):
    dma = pltpu.SemaphoreType.DMA
    others = max(1, n_tp // CORES - 1)
    pl.run_scoped(
        functools.partial(layer, n_sp, n_tp, cols, n_in, n_out, widths, refs),
        dma((2,)), dma((1,)), dma((n_sp, others)),
    )


def local(
    n_sp, n_tp, tokens_in, norm_gain, query_weight, key_weight, value_weight, pool_weight,
    sink_logit, pool_gain, attention_out_weight, pool_out_weight,
):
    rows, depth = tokens_in.shape
    seq = rows * n_tp
    ins = [query_weight, key_weight, value_weight, pool_weight]
    outs = [attention_out_weight, pool_out_weight]
    widths = tuple(w.shape[1] for w in ins)
    if widths[1] % 128:
        ins = [ins[0], jnp.concatenate(ins[1:3], axis=1), ins[3]]
    cols = math.gcd(n_sp, max(1, n_tp // CORES))
    chips = n_tp // CORES
    k_in, out_cols = ins[0].shape[0], outs[0].shape[1]
    width, others = sum(widths), max(1, chips - 1)
    qw, kw, vw, pw = widths
    vmem = pl.BlockSpec(memory_space=pltpu.VMEM)
    hbm = pl.BlockSpec(memory_space=pl.ANY)
    return pl.pallas_call(
        functools.partial(kernel, n_sp, n_tp, cols, len(ins), len(outs), widths),
        out_shape=pltpu.VMEM((rows, depth), BF16),
        in_specs=[hbm] * (4 + len(ins) + len(outs)),
        out_specs=vmem,
        scratch_shapes=[
            pltpu.VMEM((rows, depth), BF16),
            pltpu.VMEM((n_sp, seq, depth // n_sp), BF16),
            pltpu.VMEM((n_sp, k_in, qw), BF16),
            pltpu.VMEM((n_sp, k_in, kw + vw), BF16),
            pltpu.VMEM((n_sp, k_in, pw), BF16),
            pltpu.VMEM((n_sp, outs[0].shape[0], out_cols), BF16),
            pltpu.VMEM((n_sp, outs[1].shape[0], out_cols), BF16),
            pltpu.VMEM((seq, width), F32),
            pltpu.VMEM((seq + WINDOW, width), BF16),
            pltpu.VMEM((seq, qw + pw), BF16),
            pltpu.VMEM((n_sp, 8, pw), F32),
            pltpu.VMEM((seq // WINDOW, 8, pw), F32),
            pltpu.VMEM((8, pw), F32),
            pltpu.VMEM((n_sp, others, rows, out_cols), BF16),
            pltpu.VMEM((n_sp, others, rows, out_cols), BF16),
            pltpu.VMEM((n_sp, rows, out_cols), BF16),
            pltpu.VMEM((n_sp, rows, out_cols), BF16),
            pltpu.VMEM((n_sp, others, rows, out_cols), BF16),
            pltpu.VMEM((n_sp, others, rows, out_cols), BF16),
            pltpu.VMEM((n_sp, others, rows, out_cols), F32),
            pltpu.VMEM((n_sp, rows, out_cols), F32),
            pltpu.VMEM((1, depth), F32),
            pltpu.VMEM((1, pw), F32),
            pltpu.SMEM(sink_logit.shape, F32),
        ],
        compiler_params=pltpu.CompilerParams(
            collective_id=0, has_side_effects=True, vmem_limit_bytes=58 << 20
        ),
    )(
        tokens_in, norm_gain.reshape(1, -1), sink_logit, pool_gain.reshape(1, -1), *ins, *outs
    )


def solution(mesh):
    in_specs = (
        P(("sp", "tp"), None), P(), P("sp", "tp"), P("sp", "tp"), P("sp", "tp"), P("sp", "tp"),
        P("tp"), P("tp"), P("tp", "sp"), P("tp", "sp"),
    )
    out_specs = P(("sp", "tp"), None)
    return jax.shard_map(
        functools.partial(local, mesh.shape["sp"], mesh.shape["tp"]),
        mesh=mesh, in_specs=in_specs, out_specs=out_specs, check_vma=False,
    )
```

time: 67.3 us -> 64.2 us (0.954); the launches traced: 66 us -> 63.9 us
  Pallas kernels: 65.1 us -> 63 us
    pallas_call x1, Pallas kernels: 65.1 us -> 63 us  [local(): pl.pallas_call(functools.partial(kernel, n_sp, n_tp, cols, len(ins), len(...]
where the time goes in v4:
time: 64.2 us; the launch traced here: 63.9 us
  Pallas kernels  63 us (98%)
  local copies, waits for them, and re-layouts  0.88 us (1%)
    pallas_call x1, Pallas kernels, local(): pl.pallas_call(functools.partial(kernel, n_sp, n_tp, cols, len(ins), len(...  63 us

profile of v4, /device:TPU:0, one launch (start us, length us, event | category | flops | bytes accessed | tf_op | source)
XLA Modules:
  0.0 63.9 jit_solution(15921565493793142052)
XLA Ops:
  0.0 63.0 %shard_map.100 = bf16[192,2048]{1,0:T(8,128)(2,1)S(1)} custom-call(bf16[192,2048]{1,0:T(8,128)(2,1)} %refs_0_.1, f32[1,2048]{1,0:T(1,128)} %bitcast.2, f32[4]{0:T(128)} %refs_2_.1, f32[1,256]{1,0:T(1,128)} %bitcast.3, bf16[256,256]{1,0:T(8,128)(2,1)} %refs_4_.1, bf16[256,128]{1,0:T(8,128)(2,1)} %refs_5_.1, bf16[256,128]{1,0:T(8,128)(2,1)} %refs_6_.1, ...), custom_call_target="tpu_custom_call" | custom-call | tf_op jit(solution)/shard_map/pallas_call | solution.py:757
  63.0 0.9 %copy.12 = bf16[192,2048]{1,0:T(8,128)(2,1)} copy(bf16[192,2048]{1,0:T(8,128)(2,1)S(1)} %shard_map.100) | data formatting | bytes 1572864

commit v5 on v4

--- a/solution.py
+++ b/solution.py
@@ -632,18 +632,18 @@
         finish(second)
         attend_later_blocks(near_blocks)
         spread_b.forward_next()
+        spread_a.take(0)
+        spread_b.take(0)
+        multiply_far(third)
         attend_first_block(near_blocks)
+        finish(third)
         if last >= 2:
             spread_b.forward(2, at_end)
-        spread_a.take(0)
-        spread_b.take(0)
         spread_b.forward_side(z == last)
         spread_a.forward_side(z == last)
-        multiply_far(third)
-        pool(near_blocks)
-        finish(third)
         fourth = column(2) if last >= 2 else []
         multiply_far(fourth)
+        pool(near_blocks)
         multiply_near(first)
         finish(fourth)
 
@@ -662,15 +662,14 @@
             spread_a.forward(3)
         spread_b.forward_side(z == 0)
         spread_a.forward_side(z == 0)
-        multiply_near(second)
         if last >= 3:
             spread_b.forward(3)
-        left = third + fourth
+        left = second + third + fourth
         for h in range(3, last + 1):
             multiply_far(column(h))
-            multiply_near(left[:1])
+            multiply_near(left[:2])
             finish(column(h))
-            left = left[1:] + column(h)
+            left = left[2:] + column(h)
         for h in range(2, last):
             spread_a.take(h)
             spread_b.take(h)

time: 64.2 us -> 63.9 us (level)
  no operation moved by 1% of the time
where the time goes in v5:
time: 63.9 us; the launch traced here: 63.8 us
  Pallas kernels  62.9 us (98%)
  local copies, waits for them, and re-layouts  0.88 us (1%)
    pallas_call x1, Pallas kernels, local(): pl.pallas_call(functools.partial(kernel, n_sp, n_tp, cols, len(ins), len(...  62.9 us

profile of v5, /device:TPU:0, one launch (start us, length us, event | category | flops | bytes accessed | tf_op | source)
XLA Modules:
  0.0 63.8 jit_solution(9272161780806635416)
XLA Ops:
  0.0 62.9 %shard_map.100 = bf16[192,2048]{1,0:T(8,128)(2,1)S(1)} custom-call(bf16[192,2048]{1,0:T(8,128)(2,1)} %refs_0_.1, f32[1,2048]{1,0:T(1,128)} %bitcast.2, f32[4]{0:T(128)} %refs_2_.1, f32[1,256]{1,0:T(1,128)} %bitcast.3, bf16[256,256]{1,0:T(8,128)(2,1)} %refs_4_.1, bf16[256,128]{1,0:T(8,128)(2,1)} %refs_5_.1, bf16[256,128]{1,0:T(8,128)(2,1)} %refs_6_.1, ...), custom_call_target="tpu_custom_call" | custom-call | tf_op jit(solution)/shard_map/pallas_call | solution.py:756
  62.9 0.9 %copy.12 = bf16[192,2048]{1,0:T(8,128)(2,1)} copy(bf16[192,2048]{1,0:T(8,128)(2,1)S(1)} %shard_map.100) | data formatting | bytes 1572864

commit v6 on v5

--- a/solution.py
+++ b/solution.py
@@ -500,7 +500,7 @@
 
         def attend_later_blocks(firsts):
             for first in firsts:
-                pl.loop(1, span)(lambda i, first=first: attend(first + i))
+                pl.loop(1, span, unroll=2 if span % 2 else 1)(lambda i, first=first: attend(first + i))
 
         def attend_first_block(firsts):
             for first in firsts:

time: 63.9 us -> 63.9 us (level)
  no operation moved by 1% of the time
where the time goes in v6:
time: 63.9 us; the launch traced here: 63.8 us
  Pallas kernels  62.9 us (98%)
  local copies, waits for them, and re-layouts  0.88 us (1%)
    pallas_call x1, Pallas kernels, local(): pl.pallas_call(functools.partial(kernel, n_sp, n_tp, cols, len(ins), len(...  62.9 us

profile of v6, /device:TPU:0, one launch (start us, length us, event | category | flops | bytes accessed | tf_op | source)
XLA Modules:
  0.0 63.8 jit_solution(18310015469248188558)
XLA Ops:
  0.0 62.9 %shard_map.100 = bf16[192,2048]{1,0:T(8,128)(2,1)S(1)} custom-call(bf16[192,2048]{1,0:T(8,128)(2,1)} %refs_0_.1, f32[1,2048]{1,0:T(1,128)} %bitcast.2, f32[4]{0:T(128)} %refs_2_.1, f32[1,256]{1,0:T(1,128)} %bitcast.3, bf16[256,256]{1,0:T(8,128)(2,1)} %refs_4_.1, bf16[256,128]{1,0:T(8,128)(2,1)} %refs_5_.1, bf16[256,128]{1,0:T(8,128)(2,1)} %refs_6_.1, ...), custom_call_target="tpu_custom_call" | custom-call | tf_op jit(solution)/shard_map/pallas_call | solution.py:756
  62.9 0.9 %copy.12 = bf16[192,2048]{1,0:T(8,128)(2,1)} copy(bf16[192,2048]{1,0:T(8,128)(2,1)S(1)} %shard_map.100) | data formatting | bytes 1572864
